TPU v7x, 512 devices: a whole 4x8x8 slice. The times are simulated.
512 devices in a mesh: ep: 32 (over z, x), tp: 16 (over y, core).
Axes of the slice: x: 4, y: 8, z: 8, core: 2. Of those that a mesh axis runs over, the one named last changes fastest.
Arguments:
- tokens: bfloat16 [4096, 4096], P('ep', 'tp'), may hold values from -6 to 6
- cotangent: bfloat16 [4096, 4096], P('ep', 'tp'), may hold values from -6 to 6
- routes: int32 [4096, 2], P('ep'), may hold values from 0 to 31, all different within a row; in each aligned block of 128 rows (0 to 127, 128 to 255, ...) at most 12 rows name the same one
- gate_weight: float32 [4096, 2], P('ep'), may hold values from 0.1 to 2.5
- w_gate: bfloat16 [32, 1024, 4096], P('ep', 'tp'), may hold values from -0.09375 to 0.09375
- w_up: bfloat16 [32, 1024, 4096], P('ep', 'tp'), may hold values from -0.09375 to 0.09375
- w_down: bfloat16 [32, 1024, 4096], P('ep', 'tp'), may hold values from -0.1875 to 0.1875
- shared_hidden: bfloat16 [4096, 1024], P('ep'), may hold values from -4 to 4
Outputs:
- tokens_grad: bfloat16 [4096, 4096], P('ep', 'tp')
- gate_grad: float32 [4096, 2], P('ep')
- w_gate_grad: float32 [32, 1024, 4096], P('ep', 'tp')
- w_up_grad: float32 [32, 1024, 4096], P('ep', 'tp')
- w_down_grad: float32 [32, 1024, 4096], P('ep', 'tp')
- shared_grad: float32 [1024, 4096], P('ep', 'tp')
Inputs may be any that keep to these rules, and one draw needn't show every extreme that they name: `routes`: each row names 2 different experts. Among the rows of one index of ep (aligned blocks of 128 rows) no expert is named more than 12 times, and in every draw some expert is named exactly 12 times in some block.
All inputs are finite; a program needn't handle non-finite values.
Results may differ from a plain program's by a relative error of at most 0.022.
Values may be sent and summed in bfloat16 or wider, within the bound.
No kernel may reach another device: no remote copies, remote signals or barrier semaphores. Data moves between devices by JAX's collectives and lax.ppermute only.
A program may use at most 64 MiB of HBM per device.

v0:
```python
import jax
import jax.numpy as jnp
from jax import lax
from jax.sharding import PartitionSpec as P


def in_one_piece(arrays, axis, dim, along):
    ends, at = ([], 0)
    for a in arrays[:-1]:
        at += a.shape[along]
        ends.append(at)
    both = jnp.concatenate(arrays, axis=along)
    return tuple(jnp.split(lax.all_gather(both, axis, axis=dim, tiled=True), ends, axis=along))


def from_everyone(array, axis):
    copies = jnp.broadcast_to(array, (lax.axis_size(axis), *array.shape))
    return lax.all_to_all(copies, axis, split_axis=0, concat_axis=0, tiled=True)


def taken_together(array, axis):
    everything = from_everyone(array, axis)
    return jnp.sum(everything, axis=0)


def in_blocks(array, dim, size):
    before, after = (array.shape[:dim], array.shape[dim + 1 :])
    return jnp.moveaxis(array.reshape(*before, size, -1, *after), dim, 0)


def sent_and_summed(array, axis, dim):
    pieces = in_blocks(array, dim, lax.axis_size(axis))
    arrived = lax.all_to_all(pieces, axis, split_axis=0, concat_axis=0, tiled=True)
    return arrived.astype(jnp.float32).sum(axis=0)


def slot_positions(flat_routes, experts):
    onehot = (flat_routes[:, None] == jnp.arange(experts, dtype=jnp.int32)[None, :]).astype(
        jnp.int32
    )
    earlier = jnp.cumsum(onehot, axis=0) - onehot
    return jnp.sum(earlier * onehot, axis=1)


def shards(tokens, cotangent, routes, gate_weight, w_gate, w_up, w_down, shared_hidden):
    tok_count, top_count = routes.shape
    experts = lax.axis_size("ep")
    capacity = 3 * tok_count * top_count // (2 * experts)
    flat_routes = routes.reshape(-1)
    positions = slot_positions(flat_routes, experts)
    token_ids = jnp.arange(tok_count * top_count, dtype=jnp.int32) // top_count
    slot_table = (
        jnp.full((experts, capacity), tok_count, jnp.int32)
        .at[flat_routes, positions]
        .set(token_ids)
    )
    weight_table = (
        jnp.zeros((experts, capacity), jnp.float32)
        .at[flat_routes, positions]
        .set(gate_weight.reshape(-1))
    )

    def place_rows(source_rows):
        padded = jnp.concatenate(
            [source_rows, jnp.zeros((1, source_rows.shape[1]), source_rows.dtype)], 0
        )
        return padded[slot_table]

    part_tokens, part_cotan, recv_weight = (
        lax.all_to_all(place_rows(tokens), "ep", split_axis=0, concat_axis=0, tiled=True),
        lax.all_to_all(place_rows(cotangent), "ep", split_axis=0, concat_axis=0, tiled=True),
        lax.all_to_all(
            weight_table.astype(jnp.bfloat16), "ep", split_axis=0, concat_axis=0, tiled=True
        ).astype(weight_table.dtype),
    )
    recv_tokens, recv_cotan = in_one_piece((part_tokens, part_cotan), "tp", 2, 0)
    row_total = experts * capacity
    width = recv_tokens.shape[2]
    contract_last = (((1,), (1,)), ((), ()))
    rows_x = recv_tokens.reshape(row_total, width)
    rows_g = recv_cotan.reshape(row_total, width)
    weight_col = recv_weight.reshape(row_total, 1)
    gate_mat = w_gate[0]
    up_mat = w_up[0]
    down_mat = w_down[0]
    pre_gate = lax.dot_general(rows_x, gate_mat, contract_last, preferred_element_type=jnp.float32)
    pre_up = lax.dot_general(rows_x, up_mat, contract_last, preferred_element_type=jnp.float32)
    sigmoid_gate = jax.nn.sigmoid(pre_gate)
    silu_gate = pre_gate * sigmoid_gate
    hidden = (silu_gate * pre_up).astype(jnp.bfloat16)
    back_hidden = lax.dot_general(
        rows_g, down_mat, contract_last, preferred_element_type=jnp.float32
    )
    gate_part = jnp.sum(hidden.astype(jnp.float32) * back_hidden, axis=1)
    scaled = weight_col * back_hidden
    grad_pre_gate = (
        scaled * pre_up * sigmoid_gate * (1.0 + pre_gate * (1.0 - sigmoid_gate))
    ).astype(jnp.bfloat16)
    grad_pre_up = (scaled * silu_gate).astype(jnp.bfloat16)
    weighted_cotan = (weight_col * rows_g.astype(jnp.float32)).astype(jnp.bfloat16)
    grad_down = jnp.dot(hidden.T, weighted_cotan, preferred_element_type=jnp.float32)
    grad_gate = jnp.dot(grad_pre_gate.T, rows_x, preferred_element_type=jnp.float32)
    grad_up = jnp.dot(grad_pre_up.T, rows_x, preferred_element_type=jnp.float32)
    partial_value = jnp.dot(grad_pre_gate, gate_mat, preferred_element_type=jnp.float32)
    partial_value = partial_value + jnp.dot(grad_pre_up, up_mat, preferred_element_type=jnp.float32)
    rounded = lax.optimization_barrier(partial_value.astype(jnp.bfloat16)).astype(jnp.float32)
    row_share = lax.psum_scatter(
        rounded.reshape(experts, capacity, width).astype(jnp.bfloat16),
        "tp",
        scatter_dimension=2,
        tiled=True,
    )
    gate_total = taken_together(gate_part.reshape(experts, capacity), "tp")
    back_rows, back_gate = (
        lax.all_to_all(row_share, "ep", split_axis=0, concat_axis=0, tiled=True),
        lax.all_to_all(
            gate_total.astype(jnp.bfloat16), "ep", split_axis=0, concat_axis=0, tiled=True
        ).astype(gate_total.dtype),
    )
    picked = back_rows[flat_routes, positions].astype(jnp.float32)
    tokens_grad = jnp.sum(picked.reshape(tok_count, top_count, -1), axis=1).astype(jnp.bfloat16)
    gate_grad = back_gate[flat_routes, positions].reshape(tok_count, top_count)
    shared_grad = sent_and_summed(
        jnp.dot(shared_hidden.T, cotangent, preferred_element_type=jnp.float32).astype(
            jnp.bfloat16
        ),
        "ep",
        0,
    )
    return (tokens_grad, gate_grad, grad_gate[None], grad_up[None], grad_down[None], shared_grad)


def solution(mesh):
    placed = (
        P("ep", "tp"),
        P("ep", "tp"),
        P("ep", None),
        P("ep", None),
        P("ep", "tp", None),
        P("ep", "tp", None),
        P("ep", "tp", None),
        P("ep", None),
    )
    return jax.shard_map(
        shards,
        mesh=mesh,
        in_specs=placed,
        out_specs=(
            P("ep", "tp"),
            P("ep", None),
            P("ep", "tp", None),
            P("ep", "tp", None),
            P("ep", "tp", None),
            P("ep", "tp"),
        ),
        check_vma=False,
    )
```

profile of v0, /device:TPU:24, one launch (start us, length us, event | category | flops | bytes accessed | tf_op | source)
XLA Modules:
  0.0 257.4 jit_solution(6371332062408701905)
XLA Ops:
  7.2 0.9 copy.35
  8.2 0.1 eq.25
  8.3 0.1 reshape.117
  8.5 0.6 reduce-window.6
  9.1 0.2 slice_reduce_fusion
  9.5 12.8 %scatter_fusion.1 = s32[32,12]{0,1:T(8,128)S(1)} fusion(s32[32,12]{0,1:T(8,128)S(1)} %broadcast_in_dim.15, s32[256]{0:T(256)S(1)} %bitcast.68, s32[256]{0:T(256)S(1)} %and_select_fusion), kind=kCustom, calls=%fused_computation.5 | custom fusion | bytes 5120 | tf_op jit(solution)/shard_map/scatter | solution.py:55
  22.4 0.8 concatenate.16
  23.3 2.0 gather_fusion
  25.3 0.7 reshape.128
  26.1 13.2 %all-to-all-start.1 = ((bf16[32,12,256]{2,1,0:T(8,128)(2,1)}), bf16[32,12,256]{2,1,0:T(8,128)(2,1)S(1)}, u32[]{:S(2)}, u32[]{:S(2)}) async-start(bf16[32,12,256]{2,1,0:T(8,128)(2,1)} %reshape.128), calls=%async_computation.1 | async-start | bytes 524288 | tf_op jit(solution)/shard_map/all_to_all | solution.py:70
  39.3 2.1 gather_fusion.1
  41.5 10.6 %all-to-all-done.1 = bf16[32,12,256]{2,1,0:T(8,128)(2,1)S(1)} async-done(((bf16[32,12,256]{2,1,0:T(8,128)(2,1)}), bf16[32,12,256]{2,1,0:T(8,128)(2,1)S(1)}, u32[]{:S(2)}, u32[]{:S(2)}) %all-to-all-start.1) | async-done | bytes 196640 | tf_op jit(solution)/shard_map/all_to_all | solution.py:70
  52.1 16.2 %all_to_all.40 = bf16[32,12,256]{2,1,0:T(8,128)(2,1)S(1)} all-to-all(bf16[32,12,256]{2,1,0:T(8,128)(2,1)S(1)} %reshape.136), channel_id=1, replica_groups=mesh['ep'=32,'tp'=16] {'ep'}, dimensions={0} | all-to-all | bytes 393216 | tf_op jit(solution)/shard_map/all_to_all | solution.py:71
  68.3 0.9 pad_maximum_fusion
  69.5 12.8 %scatter_fusion = f32[32,12]{0,1:T(8,128)S(1)} fusion(f32[32,12]{0,1:T(8,128)S(1)} %broadcast_in_dim.14, s32[256]{0:T(256)S(1)} %bitcast.69, f32[256]{0:T(256)S(1)} %reshape.157), kind=kCustom, calls=%fused_computation.4 | custom fusion | bytes 5120 | tf_op jit(solution)/shard_map/scatter | solution.py:60
  82.3 13.1 %all_to_all.41 = bf16[32,1,12]{2,1,0:T(2,128)(2,1)S(1)} all-to-all(bf16[32,1,12]{2,1,0:T(2,128)(2,1)S(1)} %copy.40), channel_id=1, replica_groups=mesh['ep'=32,'tp'=16] {'ep'}, dimensions={0} | all-to-all | bytes 1536 | tf_op jit(solution)/shard_map/all_to_all | solution.py:72
  95.6 34.7 %all-gather.2.cloned.1.call-done = bf16[64,12,4096]{2,1,0:T(8,128)(2,1)} async-done(((bf16[64,12,256]{2,1,0:T(8,128)(2,1)}), bf16[64,12,4096]{2,1,0:T(8,128)(2,1)}) %all-gather.2.cloned.1.call-update) | async-done | bytes 6291472 | tf_op jit(solution)/shard_map/all_gather | solution.py:13
  130.4 5.9 %fusion.17 = (bf16[32,12,4096]{2,1,0:T(8,128)(2,1)}, bf16[32,12,4096]{2,1,0:T(8,128)(2,1)}) fusion(bf16[64,12,4096]{2,1,0:T(8,128)(2,1)} %all-gather.2.cloned.1.call-done), kind=kLoop, calls=%fused_computation.55 | loop fusion | bytes 12582912 | tf_op jit(solution)/shard_map/split | solution.py:13
  136.3 5.6 %reshape.121 = bf16[384,4096]{1,0:T(8,128)(2,1)} reshape(bf16[32,12,4096]{2,1,0:T(8,128)(2,1)} %get-tuple-element.29) | data formatting | bytes 6291456 | tf_op jit(solution)/shard_map/reshape | solution.py:80
  141.9 3.1 %fusion.3 = f32[384,64]{0,1:T(8,128)S(1)} fusion(bf16[384,4096]{1,0:T(8,128)(2,1)} %reshape.121, bf16[1,64,4096]{2,1,0:T(8,128)(2,1)S(1)} %copy-done), kind=kOutput, calls=%fused_computation.17 | convolution fusion | flops 201326592 | bytes 3768320 | tf_op jit(solution)/shard_map/dot_general | solution.py:86
  145.0 1.1 fusion.6
  146.1 5.6 %reshape.120 = bf16[384,4096]{1,0:T(8,128)(2,1)} reshape(bf16[32,12,4096]{2,1,0:T(8,128)(2,1)} %get-tuple-element.28) | data formatting | bytes 6291456 | tf_op jit(solution)/shard_map/reshape | solution.py:81
  151.8 3.0 %multiply_reduce_fusion = (f32[384]{0:T(512)S(1)}, bf16[384,64]{0,1:T(8,128)(2,1)S(1)}, bf16[384,64]{0,1:T(8,128)(2,1)S(1)}, bf16[384,64]{0,1:T(8,128)(2,1)S(1)}) fusion(f32[384,64]{0,1:T(8,128)S(1)} %fusion.6, f32[384,64]{0,1:T(8,128)S(1)} %fusion.3, f32[384]{0:T(512)S(1)} %reshape.125, bf16[384,4096]{1,0:T(8,128)(2,1)} %reshape.120, ...), kind=kOutput, calls=%fused_computation.24 | convolution fusion | flops 201793152 | bytes 4017152 | tf_op jit(solution)/shard_map/dot_general | solution.py:91
  154.8 1.0 fusion.1
  155.8 2.7 %add_convert_fusion = bf16[384,4096]{1,0:T(8,128)(2,1)} fusion(f32[384,4096]{1,0:T(8,128)S(1)} %fusion.1, bf16[384,64]{0,1:T(8,128)(2,1)S(1)} %get-tuple-element.31, bf16[1,64,4096]{2,1,0:T(8,128)(2,1)S(1)} %copy-done.2), kind=kOutput, calls=%fused_computation.7 | convolution fusion | flops 204472320 | bytes 10010624 | tf_op jit(solution)/shard_map/dot_general | solution.py:105
  158.5 5.5 %convert_element_type.82 = bf16[32,12,4096]{2,1,0:T(8,128)(2,1)} reshape(bf16[384,4096]{1,0:T(8,128)(2,1)} %add_convert_fusion) | data formatting | bytes 6291456 | tf_op jit(solution)/shard_map/convert_element_type | solution.py:108
  164.0 0.9 copy-done.4
  165.0 0.3 convolution_convert_fusion
  165.3 27.4 %all_to_all.42 = bf16[32,32,256]{2,1,0:T(8,128)(2,1)S(1)} all-to-all(bf16[32,32,256]{2,1,0:T(8,128)(2,1)S(1)} %bitcast.72), channel_id=1, replica_groups=mesh['ep'=32,'tp'=16] {'ep'}, dimensions={0} | all-to-all | bytes 1048576 | tf_op jit(solution)/shard_map/all_to_all | solution.py:33
  192.7 0.7 convert_reduce_fusion
  193.6 0.7 reshape.179
  194.3 5.7 %all-to-all-start.4 = ((f32[16,1,384]{2,1,0:T(1,128)}), f32[16,1,384]{2,1,0:T(1,128)S(1)}, u32[]{:S(2)}, u32[]{:S(2)}) async-start(f32[16,1,384]{2,1,0:T(1,128)} %reshape.179), calls=%async_computation.5 | async-start | bytes 49152 | tf_op jit(solution)/shard_map/all_to_all | solution.py:18
  200.0 3.7 %convolution_bitcast_fusion = f32[1,64,4096]{2,1,0:T(8,128)} fusion(bf16[384,64]{0,1:T(8,128)(2,1)S(1)} %get-tuple-element.25, bf16[384,4096]{1,0:T(8,128)(2,1)} %reshape.120, f32[384]{0:T(512)S(1)} %reshape.125), kind=kOutput, calls=%fused_computation.8 | convolution fusion | flops 206045184 | bytes 4244992 | tf_op jit(solution)/shard_map/dot_general | solution.py:101
  203.8 0.8 all-to-all-done.4
  204.6 0.5 broadcast.198
  205.1 0.7 reduce.7
  205.9 0.7 copy.44
  206.6 4.6 %all-to-all-start.5 = ((bf16[32,1,12]{2,1,0:T(2,128)(2,1)}), bf16[32,1,12]{2,1,0:T(2,128)(2,1)S(1)}, u32[]{:S(2)}, u32[]{:S(2)}) async-start(bf16[32,1,12]{2,1,0:T(2,128)(2,1)} %copy.44), calls=%async_computation.6 | async-start | bytes 32768 | tf_op jit(solution)/shard_map/all_to_all | solution.py:116
  211.2 3.6 %convolution_bitcast_fusion.1 = f32[1,64,4096]{2,1,0:T(8,128)} fusion(bf16[384,64]{0,1:T(8,128)(2,1)S(1)} %get-tuple-element.31, bf16[384,4096]{1,0:T(8,128)(2,1)} %reshape.121), kind=kOutput, calls=%fused_computation.9 | convolution fusion | flops 201326592 | bytes 4243456 | tf_op jit(solution)/shard_map/dot_general | solution.py:103
  214.8 6.1 %all-to-all-done.5 = bf16[32,1,12]{2,1,0:T(2,128)(2,1)S(1)} async-done(((bf16[32,1,12]{2,1,0:T(2,128)(2,1)}), bf16[32,1,12]{2,1,0:T(2,128)(2,1)S(1)}, u32[]{:S(2)}, u32[]{:S(2)}) %all-to-all-start.5) | async-done | bytes 800 | tf_op jit(solution)/shard_map/all_to_all | solution.py:116
  220.9 5.6 %reduce-scatter.2.cloned.1.call-done = bf16[32,12,256]{2,1,0:T(8,128)(2,1)} async-done(((bf16[32,12,4096]{2,1,0:T(8,128)(2,1)}), bf16[32,12,256]{2,1,0:T(8,128)(2,1)}) %reduce-scatter.2.cloned.1.call-update) | async-done | bytes 196624 | tf_op jit(solution)/shard_map/reduce_scatter | solution.py:107
  226.5 9.8 %all-to-all-start.3 = ((bf16[32,12,256]{2,1,0:T(8,128)(2,1)}), bf16[32,12,256]{2,1,0:T(8,128)(2,1)S(1)}, u32[]{:S(2)}, u32[]{:S(2)}) async-start(bf16[32,12,256]{2,1,0:T(8,128)(2,1)} %reduce-scatter.2.cloned.1.call-done), calls=%async_computation.4 | async-start | bytes 524288 | tf_op jit(solution)/shard_map/all_to_all | solution.py:115
  236.3 3.5 %convolution_bitcast_fusion.2 = f32[1,64,4096]{2,1,0:T(8,128)} fusion(bf16[384,64]{0,1:T(8,128)(2,1)S(1)} %get-tuple-element.30, bf16[384,4096]{1,0:T(8,128)(2,1)} %reshape.121), kind=kOutput, calls=%fused_computation.10 | convolution fusion | flops 201326592 | bytes 4243456 | tf_op jit(solution)/shard_map/dot_general | solution.py:102
  239.9 1.9 gather_fusion.3
  242.0 0.6 copy.46
  242.6 5.3 %all-to-all-done.3 = bf16[32,12,256]{2,1,0:T(8,128)(2,1)S(1)} async-done(((bf16[32,12,256]{2,1,0:T(8,128)(2,1)}), bf16[32,12,256]{2,1,0:T(8,128)(2,1)S(1)}, u32[]{:S(2)}, u32[]{:S(2)}) %all-to-all-start.3) | async-done | bytes 196640 | tf_op jit(solution)/shard_map/all_to_all | solution.py:115
  247.9 1.6 gather_fusion.2
  249.6 1.0 reduce_sum.52
  (47 shorter events, 1.8 us)
Async XLA Ops:
  7.2 134.7 %copy-start = (bf16[1,64,4096]{2,1,0:T(8,128)(2,1)S(1)}, bf16[1,64,4096]{2,1,0:T(8,128)(2,1)}, u32[]{:S(2)}) copy-start(bf16[1,64,4096]{2,1,0:T(8,128)(2,1)} %param.12) | copy-start | bytes 1572868
  7.2 32.1 %copy-start.5 = (bf16[128,256]{1,0:T(8,128)(2,1)S(1)}, bf16[128,256]{1,0:T(8,128)(2,1)}, u32[]{:S(2)}) copy-start(bf16[128,256]{1,0:T(8,128)(2,1)} %param.9) | copy-start | bytes 196612
  25.3 43.9 %copy-start.6 = (f32[128,2]{0,1:T(2,128)S(1)}, f32[128,2]{0,1:T(2,128)}, u32[]{:S(2)}) copy-start(f32[128,2]{0,1:T(2,128)} %param.11) | copy-start | bytes 3076
  26.1 26.0 %all-to-all-start.1 = ((bf16[32,12,256]{2,1,0:T(8,128)(2,1)}), bf16[32,12,256]{2,1,0:T(8,128)(2,1)S(1)}, u32[]{:S(2)}, u32[]{:S(2)}) async-start(bf16[32,12,256]{2,1,0:T(8,128)(2,1)} %reshape.128), calls=%async_computation.1 | async-start | bytes 524288 | tf_op jit(solution)/shard_map/all_to_all | solution.py:70
  39.3 91.1 %all-gather.2.cloned.1.call-start = ((), (), s32[]{:S(2)}) async-start(), calls=%async_computation.8 | async-start | bytes 8912896 | tf_op jit(solution)/shard_map/all_gather | solution.py:13
  69.1 157.4 %reduce-scatter.2.cloned.1.call-start = ((), (), s32[]{:S(2)}) async-start(), calls=%async_computation.9 | async-start | bytes 4456448 | tf_op jit(solution)/shard_map/reduce_scatter | solution.py:107
  141.9 3.1 %copy-start.1 = (bf16[384,4096]{1,0:T(8,128)(2,1)S(1)}, bf16[384,4096]{1,0:T(8,128)(2,1)}, u32[]{:S(2)}) copy-start(bf16[384,4096]{1,0:T(8,128)(2,1)} %reshape.121) | copy-start | bytes 9437188
  141.9 3.1 %copy-start.2 = (bf16[1,64,4096]{2,1,0:T(8,128)(2,1)S(1)}, bf16[1,64,4096]{2,1,0:T(8,128)(2,1)}, u32[]{:S(2)}) copy-start(bf16[1,64,4096]{2,1,0:T(8,128)(2,1)} %param.13) | copy-start | bytes 1572868
  146.1 5.6 %copy-start.3 = (bf16[1,64,4096]{2,1,0:T(8,128)(2,1)S(1)}, bf16[1,64,4096]{2,1,0:T(8,128)(2,1)}, u32[]{:S(2)}) copy-start(bf16[1,64,4096]{2,1,0:T(8,128)(2,1)} %param.14) | copy-start | bytes 1572868
  164.0 0.9 copy-start.4
  194.3 10.3 %all-to-all-start.4 = ((f32[16,1,384]{2,1,0:T(1,128)}), f32[16,1,384]{2,1,0:T(1,128)S(1)}, u32[]{:S(2)}, u32[]{:S(2)}) async-start(f32[16,1,384]{2,1,0:T(1,128)} %reshape.179), calls=%async_computation.5 | async-start | bytes 49152 | tf_op jit(solution)/shard_map/all_to_all | solution.py:18
  206.6 14.3 %all-to-all-start.5 = ((bf16[32,1,12]{2,1,0:T(2,128)(2,1)}), bf16[32,1,12]{2,1,0:T(2,128)(2,1)S(1)}, u32[]{:S(2)}, u32[]{:S(2)}) async-start(bf16[32,1,12]{2,1,0:T(2,128)(2,1)} %copy.44), calls=%async_computation.6 | async-start | bytes 32768 | tf_op jit(solution)/shard_map/all_to_all | solution.py:116
  226.5 21.4 %all-to-all-start.3 = ((bf16[32,12,256]{2,1,0:T(8,128)(2,1)}), bf16[32,12,256]{2,1,0:T(8,128)(2,1)S(1)}, u32[]{:S(2)}, u32[]{:S(2)}) async-start(bf16[32,12,256]{2,1,0:T(8,128)(2,1)} %reduce-scatter.2.cloned.1.call-done), calls=%async_computation.4 | async-start | bytes 524288 | tf_op jit(solution)/shard_map/all_to_all | solution.py:115
Sparse Core Ops, SparseCore 0:
  69.3 61.0 all-gather.1
  164.2 62.2 reduce-scatter.1
where the time goes:
time: 262 us; the launch traced here: 257 us
  local copies, waits for them, and re-layouts  63.7 us (24%)
  waiting for transfers between devices  63.1 us (24%)
  blocking collectives  56.7 us (22%)
  starting transfers between devices  33.4 us (13%)
  matrix products  22.1 us (8%)
  between operations  14.4 us (5%)
  other arithmetic  4.05 us (2%)
    all_gather x1, waiting for transfers between devices, in_one_piece(): lax.all_gather(both, axis, axis=dim, tiled=True)  34.7 us
    all_to_all x1, blocking collectives, sent_and_summed(): lax.all_to_all(pieces, axis, split_axis=0, concat_axis=0, tiled=True)  27.4 us
    all_to_all x1, blocking collectives, shards(): lax.all_to_all(place_rows(cotangent), 'ep', split_axis=0, concat_axis=0,...  16.2 us
    all_to_all x1, starting transfers between devices, shards(): lax.all_to_all(place_rows(tokens), 'ep', split_axis=0, concat_axis=0, til...  13.2 us
    all_to_all x1, blocking collectives, shards(): lax.all_to_all(weight_table.astype(jnp.bfloat16), 'ep', split_axis=0, con...  13.1 us
    scatter x1, local copies, waits for them, and re-layouts, shards(): slot_table = jnp.full((experts, capacity), tok_count, jnp.int32).at[flat_...  12.8 us
    scatter x1, local copies, waits for them, and re-layouts, shards(): weight_table = jnp.zeros((experts, capacity), jnp.float32).at[flat_routes...  12.8 us
    all_to_all x1, waiting for transfers between devices, shards(): lax.all_to_all(place_rows(tokens), 'ep', split_axis=0, concat_axis=0, til...  10.6 us
  transfers between devices with their start and end apart: 6, of which 6 were waited for; matrix products, arithmetic and copies ran while one was open for 13% of the time, Pallas kernels for 0%

commit v1 on v0

v1 whole, which is shorter than its diff:
```python
import jax
import jax.numpy as jnp
from jax import lax
from jax.experimental import pallas as pl
from jax.experimental.pallas import tpu as pltpu
from jax.sharding import Mesh, PartitionSpec as P

TOK, TOP, EXPERTS, CAP = 128, 2, 32, 12
SLOTS = EXPERTS * CAP
ROWS = 2 * SLOTS
PAIR = 2 * CAP
WIDTH = 256
NY = 8
HALF = NY * WIDTH
HID = 64
BACK = SLOTS + 16
EP = ("z", "x")
F32, BF16, I32 = jnp.float32, jnp.bfloat16, jnp.int32


def iota(shape, dim):
    return lax.broadcasted_iota(I32, shape, dim)


def slot_codes(rt):
    ids = iota((EXPERTS, TOK), 0)
    first, second = rt[0:1, :] == ids, rt[1:2, :] == ids
    hot = jnp.where(first, 1.0, 0.0) + jnp.where(second, 1.0, 0.0)
    upper = jnp.where(iota((TOK, TOK), 0) < iota((TOK, TOK), 1), 1.0, 0.0)
    rank = jnp.dot(hot.astype(BF16), upper.astype(BF16), preferred_element_type=F32)
    return jnp.where(hot > 0.5, rank, -1.0), first, second


def dispatch_kernel(rt_ref, gw_ref, tok_ref, cot_ref, out_ref):
    code, first, second = slot_codes(rt_ref[...])
    gw = gw_ref[...]
    weight = jnp.where(first, gw[0:1, :], 0.0) + jnp.where(second, gw[1:2, :], 0.0)
    shape = (EXPERTS, PAIR, TOK)
    code3 = jnp.broadcast_to(code[:, None, :], shape)
    weight3 = jnp.broadcast_to(weight[:, None, :], shape)
    at = iota(shape, 1)
    atf = at.astype(F32)
    sel_x = jnp.where(code3 == atf, jnp.where(at < CAP, 1.0, 0.0), 0.0)
    sel_g = jnp.where(code3 == atf - float(CAP), jnp.where(at >= CAP, 1.0, 0.0), 0.0)
    scale = jnp.sum(sel_g * weight3 + sel_x, axis=2, keepdims=True).reshape(ROWS, 1)
    select = jnp.concatenate(
        [sel_x.reshape(ROWS, TOK).astype(BF16), sel_g.reshape(ROWS, TOK).astype(BF16)], axis=1
    )
    source = jnp.concatenate([tok_ref[...], cot_ref[...]], axis=0)
    rows = jnp.dot(select, source, preferred_element_type=F32)
    out_ref[...] = (rows * scale).astype(BF16).reshape(EXPERTS, PAIR, WIDTH)


def dispatch(rt, gw, tokens, cotangent):
    return pl.pallas_call(
        dispatch_kernel,
        out_shape=jax.ShapeDtypeStruct((EXPERTS, PAIR, WIDTH), BF16),
        name="dispatch",
    )(rt, gw, tokens, cotangent)


def split_kernel(c_ref, wg_ref, wu_ref, wd_ref, out_ref):
    off = pl.multiple_of((1 - c_ref[0]) * WIDTH, WIDTH)
    out_ref[0] = wg_ref[:, pl.ds(off, WIDTH)]
    out_ref[1] = wu_ref[:, pl.ds(off, WIDTH)]
    out_ref[2] = wd_ref[:, pl.ds(off, WIDTH)]


def weight_spec():
    return pl.BlockSpec((HID, 2 * WIDTH), lambda i: (0, i))


def scalar_spec():
    return pl.BlockSpec(memory_space=pltpu.SMEM)


def whole(shape):
    return pl.BlockSpec(shape, lambda i: (0,) * len(shape))


def other_half(core, wg, wu, wd):
    return pl.pallas_call(
        split_kernel,
        grid=(NY,),
        in_specs=[scalar_spec()] + [weight_spec()] * 3,
        out_specs=pl.BlockSpec((3, HID, WIDTH), lambda i: (0, 0, i)),
        out_shape=jax.ShapeDtypeStruct((3, HID, HALF), BF16),
        name="other_half",
    )(core, wg, wu, wd)


def forward_kernel(c_ref, xg_ref, wg_ref, wu_ref, wd_ref, wr_ref, out_ref, acc_ref):
    step = pl.program_id(0)
    off = pl.multiple_of(c_ref[0] * WIDTH, WIDTH)
    mats = jnp.concatenate(
        [
            wg_ref[:, pl.ds(off, WIDTH)],
            wr_ref[0],
            wu_ref[:, pl.ds(off, WIDTH)],
            wr_ref[1],
            wd_ref[:, pl.ds(off, WIDTH)],
            wr_ref[2],
        ],
        axis=0,
    )
    part = lax.dot_general(
        xg_ref[0], mats, (((1,), (1,)), ((), ())), preferred_element_type=F32
    )

    @pl.when(step == 0)
    def _():
        acc_ref[...] = part

    @pl.when(step > 0)
    def _():
        acc_ref[...] = acc_ref[...] + part

    @pl.when(step == NY - 1)
    def _():
        for s in range(EXPERTS):
            out_ref[s * CAP : (s + 1) * CAP, 0 : 4 * HID] = acc_ref[
                s * PAIR : s * PAIR + CAP, 0 : 4 * HID
            ]
            out_ref[s * CAP : (s + 1) * CAP, 4 * HID : 6 * HID] = acc_ref[
                s * PAIR + CAP : (s + 1) * PAIR, 4 * HID : 6 * HID
            ]


def forward(core, xg, wg, wu, wd, wr):
    return pl.pallas_call(
        forward_kernel,
        grid=(NY,),
        in_specs=[scalar_spec(), pl.BlockSpec((1, ROWS, WIDTH), lambda i: (i, 0, 0))]
        + [weight_spec()] * 3
        + [pl.BlockSpec((3, HID, WIDTH), lambda i: (0, 0, i))],
        out_specs=whole((SLOTS, 6 * HID)),
        out_shape=jax.ShapeDtypeStruct((SLOTS, 6 * HID), F32),
        scratch_shapes=[pltpu.VMEM((ROWS, 6 * HID), F32)],
        name="forward",
    )(core, xg, wg, wu, wd, wr)


def backward_kernel(
    c_ref, own_ref, got_ref, wg_ref, wu_ref, wr_ref, out_ref, left_ref, grads_ref, spread_ref
):
    step = pl.program_id(0)

    @pl.when(step == 0)
    def _():
        def total(at):
            cols = slice(at * 2 * HID, (at + 1) * 2 * HID)
            return own_ref[:, cols] + pltpu.roll(got_ref[:, cols], HID, 1)

        pre_gate, pre_up, back = total(0), total(1), total(2)
        sig = 1.0 / (1.0 + jnp.exp(-pre_gate))
        silu = pre_gate * sig
        hidden = (silu * pre_up).astype(BF16).astype(F32)
        grad_gate = back * pre_up * sig * (1.0 + pre_gate * (1.0 - sig))
        grad_up = back * silu
        both = jnp.concatenate([grad_gate, grad_up], axis=1)
        grads_ref[...] = both.astype(BF16)
        gate = jnp.sum(hidden * back, axis=1, keepdims=True)
        row = iota((SLOTS, WIDTH), 0)
        lane = iota((SLOTS, WIDTH), 1)
        src = (row * 5462) >> 16
        want = (src >> 4) * TOK + row - src * CAP
        table = jnp.where(lane == want, jnp.broadcast_to(gate, (SLOTS, WIDTH)), 0.0)
        col = iota((16, SLOTS), 1)
        picks = jnp.where(((col * 5462) >> 16) % 16 == iota((16, SLOTS), 0), 1.0, 0.0)
        packed = jnp.dot(picks.astype(BF16), table.astype(BF16), preferred_element_type=F32)
        for y in range(NY):
            out_ref[y, SLOTS:BACK, :] = packed.astype(BF16)
        spread_ref[...] = jnp.zeros((ROWS, 6 * HID), F32)
        for s in range(EXPERTS):
            spread_ref[s * PAIR : s * PAIR + CAP, 0 : 4 * HID] = both[s * CAP : (s + 1) * CAP, :]
            spread_ref[s * PAIR + CAP : (s + 1) * PAIR, 4 * HID : 6 * HID] = hidden[
                s * CAP : (s + 1) * CAP, :
            ]
        flipped = spread_ref[...].T.astype(BF16)
        for at in range(3):
            left_ref[0, at * HID : (at + 1) * HID, :] = flipped[2 * at * HID : (2 * at + 1) * HID]
            left_ref[1, at * HID : (at + 1) * HID, :] = flipped[
                (2 * at + 1) * HID : (2 * at + 2) * HID
            ]

    off = pl.multiple_of(c_ref[0] * WIDTH, WIDTH)
    mats = jnp.concatenate(
        [wg_ref[:, pl.ds(off, WIDTH)], wr_ref[0], wu_ref[:, pl.ds(off, WIDTH)], wr_ref[1]], axis=0
    )
    rows = jnp.dot(grads_ref[...], mats, preferred_element_type=F32)
    out_ref[step, 0:SLOTS, :] = rows.astype(BF16)


def backward(core, own, got, wg, wu, wr):
    return pl.pallas_call(
        backward_kernel,
        grid=(NY,),
        in_specs=[scalar_spec(), whole((SLOTS, 6 * HID)), whole((SLOTS, 6 * HID))]
        + [weight_spec()] * 2
        + [pl.BlockSpec((2, HID, WIDTH), lambda i: (0, 0, i))],
        out_specs=(whole((NY, BACK, WIDTH)), whole((2, 3 * HID, ROWS))),
        out_shape=(
            jax.ShapeDtypeStruct((NY, BACK, WIDTH), BF16),
            jax.ShapeDtypeStruct((2, 3 * HID, ROWS), BF16),
        ),
        scratch_shapes=[pltpu.VMEM((SLOTS, 4 * HID), BF16), pltpu.VMEM((ROWS, 6 * HID), F32)],
        name="backward",
    )(core, own, got, wg, wu, wr)


def partner_kernel(left_ref, xg_ref, out_ref):
    out_ref[...] = jnp.dot(left_ref[0], xg_ref[0], preferred_element_type=F32).astype(BF16)


def partner_grads(left, xg):
    return pl.pallas_call(
        partner_kernel,
        grid=(NY,),
        in_specs=[
            pl.BlockSpec((1, 3 * HID, ROWS), lambda i: (1, 0, 0)),
            pl.BlockSpec((1, ROWS, WIDTH), lambda i: (i, 0, 0)),
        ],
        out_specs=pl.BlockSpec((3 * HID, WIDTH), lambda i: (0, i)),
        out_shape=jax.ShapeDtypeStruct((3 * HID, HALF), BF16),
        name="partner_grads",
    )(left, xg)


def merge_kernel(c_ref, left_ref, xg_ref, got_ref, gate_ref, up_ref, down_ref):
    off = pl.multiple_of(c_ref[0] * WIDTH, WIDTH)
    away = pl.multiple_of((1 - c_ref[0]) * WIDTH, WIDTH)
    mine = jnp.dot(left_ref[0], xg_ref[0], preferred_element_type=F32)
    for at, ref in enumerate((gate_ref, up_ref, down_ref)):
        ref[:, pl.ds(off, WIDTH)] = mine[at * HID : (at + 1) * HID, :]
        ref[:, pl.ds(away, WIDTH)] = got_ref[at * HID : (at + 1) * HID, :].astype(F32)


def merged_grads(core, left, xg, got):
    return pl.pallas_call(
        merge_kernel,
        grid=(NY,),
        in_specs=[
            scalar_spec(),
            pl.BlockSpec((1, 3 * HID, ROWS), lambda i: (0, 0, 0)),
            pl.BlockSpec((1, ROWS, WIDTH), lambda i: (i, 0, 0)),
            pl.BlockSpec((3 * HID, WIDTH), lambda i: (0, i)),
        ],
        out_specs=[pl.BlockSpec((HID, 2 * WIDTH), lambda i: (0, i))] * 3,
        out_shape=[jax.ShapeDtypeStruct((HID, 2 * HALF), F32)] * 3,
        name="merged_grads",
    )(core, left, xg, got)


def reduce_kernel(got_ref, out_ref, acc_ref):
    total = got_ref[0].astype(F32)
    for y in range(1, NY):
        total = total + got_ref[y].astype(F32)
    acc_ref[...] = total
    out_ref[...] = jnp.zeros((EXPERTS, 16, WIDTH), BF16)
    for s in range(EXPERTS):
        out_ref[s, 0:CAP, :] = acc_ref[s * CAP : (s + 1) * CAP, :].astype(BF16)
        lanes = slice((s // 16) * TOK, (s // 16 + 1) * TOK)
        out_ref[s, CAP : CAP + 1, 0:TOK] = acc_ref[
            SLOTS + s % 16 : SLOTS + s % 16 + 1, lanes
        ].astype(BF16)


def reduced(got):
    return pl.pallas_call(
        reduce_kernel,
        out_shape=jax.ShapeDtypeStruct((EXPERTS, 16, WIDTH), BF16),
        scratch_shapes=[pltpu.VMEM((BACK, WIDTH), F32)],
        name="reduced",
    )(got)


def combine_kernel(rt_ref, gw_ref, back_ref, out_ref, gate_ref):
    code, first, second = slot_codes(rt_ref[...])
    shape = (EXPERTS, 16, TOK)
    code3 = jnp.broadcast_to(code[:, None, :], shape)
    select = jnp.where(code3 == iota(shape, 1).astype(F32), 1.0, 0.0)
    select = select.reshape(EXPERTS * 16, TOK).T.astype(BF16)
    back = back_ref[...]
    rows = jnp.dot(
        select, back.reshape(EXPERTS * 16, WIDTH), preferred_element_type=F32
    )
    out_ref[...] = rows.astype(BF16)
    shares = back[:, CAP, 0:TOK].astype(F32)
    mine = jnp.zeros((EXPERTS, TOK), F32)
    for p in range(CAP):
        mine = mine + jnp.where(code == float(p), shares[:, p : p + 1], 0.0)
    top = jnp.sum(jnp.where(first, mine, 0.0), axis=0, keepdims=True)
    low = jnp.sum(jnp.where(second, mine, 0.0), axis=0, keepdims=True)
    gate_ref[...] = jnp.concatenate([top, low], axis=0) / gw_ref[...]


def combine(rt, gw, back):
    return pl.pallas_call(
        combine_kernel,
        out_shape=(
            jax.ShapeDtypeStruct((TOK, WIDTH), BF16),
            jax.ShapeDtypeStruct((TOP, TOK), F32),
        ),
        name="combine",
    )(rt, gw, back)


def core_swap(value):
    return lax.ppermute(value, "c", [(0, 1), (1, 0)])


def shards(tokens, cotangent, routes, gate_weight, w_gate, w_up, w_down, shared_hidden):
    rt, gw = routes.T, gate_weight.T
    core = lax.axis_index("c").astype(I32).reshape(1)
    wg, wu, wd = w_gate[0], w_up[0], w_down[0]
    sent = dispatch(rt, gw, tokens, cotangent)
    rows = lax.all_to_all(sent, EP, split_axis=0, concat_axis=0, tiled=True)
    rows, cotangent, wg, wu, wd = lax.optimization_barrier((rows, cotangent, wg, wu, wd))
    xg = lax.all_gather(rows.reshape(ROWS, WIDTH), "y", axis=0, tiled=False)

    wr = core_swap(other_half(core, wg, wu, wd))
    shared = lax.dot_general(
        shared_hidden, cotangent, (((0,), (0,)), ((), ())), preferred_element_type=F32
    ).astype(BF16)
    shared = lax.all_to_all(
        shared.reshape(EXPERTS, -1, WIDTH), EP, split_axis=0, concat_axis=0, tiled=True
    )
    shared_grad = jnp.sum(shared.astype(F32), axis=0)
    xg, wr, shared_grad = lax.optimization_barrier((xg, wr, shared_grad))

    own = forward(core, xg, wg, wu, wd, wr)
    parts, left = backward(core, own, core_swap(own), wg, wu, wr)
    theirs = core_swap(partner_grads(left, xg))
    grads = merged_grads(core, left, xg, theirs)
    got = lax.all_to_all(parts, "y", split_axis=0, concat_axis=0, tiled=True)
    back = lax.all_to_all(reduced(got), EP, split_axis=0, concat_axis=0, tiled=True)
    tokens_grad, gate_grad = combine(rt, gw, back)
    return (tokens_grad, gate_grad.T, grads[0][None], grads[1][None], grads[2][None], shared_grad)


def solution(mesh):
    split = Mesh(mesh.devices.reshape(8, 4, 8, 2), ("z", "x", "y", "c"))
    ep, tp = ("z", "x"), ("y", "c")
    placed = (
        P(ep, tp),
        P(ep, tp),
        P(ep, None),
        P(ep, None),
        P(ep, tp, None),
        P(ep, tp, None),
        P(ep, tp, None),
        P(ep, None),
    )
    return jax.shard_map(
        shards,
        mesh=split,
        in_specs=placed,
        out_specs=(
            P(ep, tp),
            P(ep, None),
            P(ep, tp, None),
            P(ep, tp, None),
            P(ep, tp, None),
            P(ep, tp),
        ),
        check_vma=False,
    )
```

time: 262 us -> 184 us (0.70)
  the two profiles are of different devices: /device:TPU:24 before, /device:TPU:1 now
where the time goes in v1:
time: 184 us; the launch traced here: 183 us
  waiting for transfers between devices  66.6 us (36%)
  Pallas kernels  40.3 us (22%)
  starting transfers between devices  28.7 us (16%)
  blocking collectives  27.6 us (15%)
  between operations  14.1 us (8%)
  local copies, waits for them, and re-layouts  4.61 us (3%)
    all_to_all x1, waiting for transfers between devices, shards(): got = lax.all_to_all(parts, 'y', split_axis=0, concat_axis=0, tiled=True)  32.7 us
    all_to_all x1, blocking collectives, shards(): rows = lax.all_to_all(sent, EP, split_axis=0, concat_axis=0, tiled=True)  27.6 us
    all_gather x1, waiting for transfers between devices, shards(): xg = lax.all_gather(rows.reshape(ROWS, WIDTH), 'y', axis=0, tiled=False)  21.7 us
    all_to_all x1, starting transfers between devices, shards(): lax.all_to_all(reduced(got), EP, split_axis=0, concat_axis=0, tiled=True)  9.9 us
    ppermute x3, starting transfers between devices, core_swap(): return lax.ppermute(value, 'c', [(0, 1), (1, 0)])  9.67 us
    pallas_call x1, Pallas kernels, forward(): pl.pallas_call(forward_kernel, grid=(NY,), in_specs=[scalar_spec(), pl.Bl...  7.94 us
    pallas_call x1, Pallas kernels, merged_grads(): pl.pallas_call(merge_kernel, grid=(NY,), in_specs=[scalar_spec(), pl.Bloc...  7.07 us
    pallas_call x1, Pallas kernels, backward(): pl.pallas_call(backward_kernel, grid=(NY,), in_specs=[scalar_spec(), whol...  7.05 us
  transfers between devices with their start and end apart: 7, of which 5 were waited for; matrix products, arithmetic and copies ran while one was open for 1% of the time, Pallas kernels for 12%

profile of v1, /device:TPU:1, one launch (start us, length us, event | category | flops | bytes accessed | tf_op | source)
XLA Modules:
  0.0 183.0 jit_solution(10514548430167177964)
XLA Ops:
  7.2 0.0 copy-start
  7.2 0.0 copy-start.6
  7.2 0.0 all-gather.2.cloned.1.call-start
  7.2 2.1 %dispatch.1 = bf16[32,24,256]{2,1,0:T(8,128)(2,1)} custom-call(s32[2,128]{1,0:T(2,128)} %bitcast.25, f32[2,128]{1,0:T(2,128)} %bitcast.27, bf16[128,256]{1,0:T(8,128)(2,1)} %tok_ref.1, bf16[128,256]{1,0:T(8,128)(2,1)} %cot_ref.1), custom_call_target="tpu_custom_call" | custom-call | tf_op jit(solution)/shard_map/dispatch/pallas_call | solution.py:55
  9.3 27.6 %all_to_all.20 = bf16[32,24,256]{2,1,0:T(8,128)(2,1)} all-to-all(bf16[32,24,256]{2,1,0:T(8,128)(2,1)} %dispatch.1), channel_id=1, replica_groups=mesh['z'=8,'x'=4,'y'=8,'c'=2] {'z','x'}, dimensions={0} | all-to-all | bytes 786432 | tf_op jit(solution)/shard_map/all_to_all | solution.py:317
  37.0 0.0 all-gather.2.cloned.1.call-update
  37.0 0.0 copy-done
  37.0 0.0 copy-done.6
  37.0 0.3 fusion
  37.3 1.0 copy.15
  38.3 5.0 %all-to-all-start.1 = ((bf16[32,32,256]{2,1,0:T(8,128)(2,1)}), bf16[32,32,256]{2,1,0:T(8,128)(2,1)S(1)}, u32[]{:S(2)}, u32[]{:S(2)}) async-start(bf16[32,32,256]{2,1,0:T(8,128)(2,1)} %bitcast.8), calls=%async_computation.1 | async-start | bytes 1048576 | tf_op jit(solution)/shard_map/all_to_all | solution.py:325
  43.4 5.1 %other_half.1 = bf16[3,64,2048]{2,1,0:T(8,128)(2,1)} custom-call(s32[1]{0:T(128)} %bitcast.2.c_ref, bf16[64,4096]{1,0:T(8,128)(2,1)} %bitcast.16, bf16[64,4096]{1,0:T(8,128)(2,1)} %bitcast.19, bf16[64,4096]{1,0:T(8,128)(2,1)} %bitcast.22), custom_call_target="tpu_custom_call" | custom-call | tf_op jit(solution)/shard_map/other_half/pallas_call | solution.py:82
  48.5 3.6 %collective-permute-start = (bf16[3,64,2048]{2,1,0:T(8,128)(2,1)}, bf16[3,64,2048]{2,1,0:T(8,128)(2,1)S(1)}, u32[]{:S(2)}, u32[]{:S(2)}) collective-permute-start(bf16[3,64,2048]{2,1,0:T(8,128)(2,1)} %other_half.1), channel_id=1, source_target_pairs={{0,1},{1,0},{2,3},{3,2},{4,5},{5,4},{6,7},{7,6},{8,9},{9,8},{10,11... | collective-permute-start | bytes 2359304 | tf_op jit(solution)/shard_map/ppermute | solution.py:309
  52.1 6.7 %all-to-all-done.1 = bf16[32,32,256]{2,1,0:T(8,128)(2,1)S(1)} async-done(((bf16[32,32,256]{2,1,0:T(8,128)(2,1)}), bf16[32,32,256]{2,1,0:T(8,128)(2,1)S(1)}, u32[]{:S(2)}, u32[]{:S(2)}) %all-to-all-start.1) | async-done | bytes 524320 | tf_op jit(solution)/shard_map/all_to_all | solution.py:325
  58.8 0.7 convert_reduce_fusion
  59.5 0.0 collective-permute-done.wr_ref
  59.5 0.0 copy-start.2
  59.5 21.7 %all-gather.2.cloned.1.call-done.xg_ref = bf16[8,768,256]{2,1,0:T(8,128)(2,1)} async-done(((bf16[1,768,256]{2,1,0:T(8,128)(2,1)}), bf16[8,768,256]{2,1,0:T(8,128)(2,1)}) %all-gather.2.cloned.1.call-update) | async-done | bytes 3145744 | tf_op jit(solution)/shard_map/all_gather | solution.py:319
  81.2 0.0 copy-done.2
  81.2 7.9 %forward.1.own_ref = f32[384,384]{1,0:T(8,128)} custom-call(s32[1]{0:T(128)} %bitcast.2.c_ref, bf16[8,768,256]{2,1,0:T(8,128)(2,1)} %all-gather.2.cloned.1.call-done.xg_ref, bf16[64,4096]{1,0:T(8,128)(2,1)} %bitcast.17, bf16[64,4096]{1,0:T(8,128)(2,1)} %bitcast.20, bf16[64,4096]{1,0:T(8,128)(2,1)} %bitcast.23, bf16[3,64,2048]{2,1,0:T(8,128)(2,1)} %copy-done.2), custom_call_target="tpu_custom_call" | custom-call | tf_op jit(solution)/shard_map/forward/pallas_call | solution.py:130
  89.2 3.5 %collective-permute-start.1 = (f32[384,384]{1,0:T(8,128)}, f32[384,384]{1,0:T(8,128)S(1)}, u32[]{:S(2)}, u32[]{:S(2)}) collective-permute-start(f32[384,384]{1,0:T(8,128)} %forward.1.own_ref), channel_id=1, source_target_pairs={{0,1},{1,0},{2,3},{3,2},{4,5},{5,4},{6,7},{7,6},{8,9},{9,8},{10,11... | collective-permute-start | bytes 1769480 | tf_op jit(solution)/shard_map/ppermute | solution.py:309
  92.7 1.8 collective-permute-done.1.got_ref
  94.5 0.0 copy-start.5
  94.5 0.8 copy-done.5
  95.3 7.0 %backward.1 = (bf16[8,400,256]{2,1,0:T(8,128)(2,1)}, bf16[2,192,768]{2,1,0:T(8,128)(2,1)}) custom-call(s32[1]{0:T(128)} %bitcast.2.c_ref, f32[384,384]{1,0:T(8,128)} %forward.1.own_ref, f32[384,384]{1,0:T(8,128)} %copy-done.5, bf16[64,4096]{1,0:T(8,128)(2,1)} %bitcast.18, bf16[64,4096]{1,0:T(8,128)(2,1)} %bitcast.21, bf16[3,64,2048]{2,1,0:T(8,128)(2,1)} %copy-done.2), custom_call_target="tpu_custom_call" | custom-call | tf_op jit(solution)/shard_map/backward/pallas_call | solution.py:195
  102.4 4.1 %all-to-all-start.2 = ((bf16[8,400,256]{2,1,0:T(8,128)(2,1)}), bf16[8,400,256]{2,1,0:T(8,128)(2,1)S(1)}, u32[]{:S(2)}, u32[]{:S(2)}) async-start(bf16[8,400,256]{2,1,0:T(8,128)(2,1)} %get-tuple-element.28), calls=%async_computation.2 | async-start | bytes 3276800 | tf_op jit(solution)/shard_map/all_to_all | solution.py:335
  106.5 6.5 %partner_grads.1 = bf16[192,2048]{1,0:T(8,128)(2,1)} custom-call(bf16[2,192,768]{2,1,0:T(8,128)(2,1)} %get-tuple-element.31.left_ref, bf16[8,768,256]{2,1,0:T(8,128)(2,1)} %all-gather.2.cloned.1.call-done.xg_ref), custom_call_target="tpu_custom_call" | custom-call | tf_op jit(solution)/shard_map/partner_grads/pallas_call | solution.py:216
  113.0 2.6 %collective-permute-start.2 = (bf16[192,2048]{1,0:T(8,128)(2,1)}, bf16[192,2048]{1,0:T(8,128)(2,1)S(1)}, u32[]{:S(2)}, u32[]{:S(2)}) collective-permute-start(bf16[192,2048]{1,0:T(8,128)(2,1)} %partner_grads.1), channel_id=1, source_target_pairs={{0,1},{1,0},{2,3},{3,2},{4,5},{5,4},{6,7},{7,6},{8,9},{9,8},{10,11... | collective-permute-start | bytes 2359304 | tf_op jit(solution)/shard_map/ppermute | solution.py:309
  115.6 32.7 %all-to-all-done.2.got_ref = bf16[8,400,256]{2,1,0:T(8,128)(2,1)S(1)} async-done(((bf16[8,400,256]{2,1,0:T(8,128)(2,1)}), bf16[8,400,256]{2,1,0:T(8,128)(2,1)S(1)}, u32[]{:S(2)}, u32[]{:S(2)}) %all-to-all-start.2) | async-done | bytes 1638432 | tf_op jit(solution)/shard_map/all_to_all | solution.py:335
  148.3 0.0 copy-start.1
  148.3 1.2 copy-done.1
  149.5 2.5 %reduced.1 = bf16[32,16,256]{2,1,0:T(8,128)(2,1)} custom-call(bf16[8,400,256]{2,1,0:T(8,128)(2,1)} %copy-done.1), custom_call_target="tpu_custom_call" | custom-call | tf_op jit(solution)/shard_map/reduced/pallas_call | solution.py:269
  152.0 9.9 %all-to-all-start.3 = ((bf16[32,16,256]{2,1,0:T(8,128)(2,1)}), bf16[32,16,256]{2,1,0:T(8,128)(2,1)S(1)}, u32[]{:S(2)}, u32[]{:S(2)}) async-start(bf16[32,16,256]{2,1,0:T(8,128)(2,1)} %reduced.1), calls=%async_computation.3 | async-start | bytes 524288 | tf_op jit(solution)/shard_map/all_to_all | solution.py:336
  161.9 0.0 collective-permute-done.2.got_ref
  161.9 0.0 copy-start.4
  161.9 0.9 copy-done.4
  162.8 7.1 %merged_grads.1 = (f32[64,4096]{1,0:T(8,128)}, f32[64,4096]{1,0:T(8,128)}, f32[64,4096]{1,0:T(8,128)}) custom-call(s32[1]{0:T(128)} %bitcast.2.c_ref, bf16[2,192,768]{2,1,0:T(8,128)(2,1)} %get-tuple-element.31.left_ref, bf16[8,768,256]{2,1,0:T(8,128)(2,1)} %all-gather.2.cloned.1.call-done.xg_ref, bf16[192,2048]{1,0:T(8,128)(2,1)} %copy-done.4), custom_call_target="tpu_custom_call" | custom-call | tf_op jit(solution)/shard_map/merged_grads/pallas_call | solution.py:239
  169.9 3.6 %all-to-all-done.3.back_ref = bf16[32,16,256]{2,1,0:T(8,128)(2,1)S(1)} async-done(((bf16[32,16,256]{2,1,0:T(8,128)(2,1)}), bf16[32,16,256]{2,1,0:T(8,128)(2,1)S(1)}, u32[]{:S(2)}, u32[]{:S(2)}) %all-to-all-start.3) | async-done | bytes 262176 | tf_op jit(solution)/shard_map/all_to_all | solution.py:336
  173.5 0.0 copy-start.3
  173.5 0.7 copy-done.3
  174.2 2.0 %combine.1 = (bf16[128,256]{1,0:T(8,128)(2,1)}, f32[2,128]{1,0:T(2,128)}) custom-call(s32[2,128]{1,0:T(2,128)} %bitcast.26, f32[2,128]{1,0:T(2,128)} %bitcast.28, bf16[32,16,256]{2,1,0:T(8,128)(2,1)} %copy-done.3), custom_call_target="tpu_custom_call" | custom-call | tf_op jit(solution)/shard_map/combine/pallas_call | solution.py:298
Async XLA Ops:
  7.2 29.8 %copy-start = (bf16[128,1024]{1,0:T(8,128)(2,1)S(1)}, bf16[128,1024]{1,0:T(8,128)(2,1)}, u32[]{:S(2)}) copy-start(bf16[128,1024]{1,0:T(8,128)(2,1)} %param.15) | copy-start | bytes 786436
  7.2 29.8 %copy-start.6 = (bf16[128,256]{1,0:T(8,128)(2,1)S(1)}, bf16[128,256]{1,0:T(8,128)(2,1)}, u32[]{:S(2)}) copy-start(bf16[128,256]{1,0:T(8,128)(2,1)} %cot_ref.1) | copy-start | bytes 196612
  7.2 74.0 %all-gather.2.cloned.1.call-start = ((), (), s32[]{:S(2)}) async-start(), calls=%async_computation.4 | async-start | bytes 3538944 | tf_op jit(solution)/shard_map/all_gather | solution.py:319
  38.3 20.5 %all-to-all-start.1 = ((bf16[32,32,256]{2,1,0:T(8,128)(2,1)}), bf16[32,32,256]{2,1,0:T(8,128)(2,1)S(1)}, u32[]{:S(2)}, u32[]{:S(2)}) async-start(bf16[32,32,256]{2,1,0:T(8,128)(2,1)} %bitcast.8), calls=%async_computation.1 | async-start | bytes 1048576 | tf_op jit(solution)/shard_map/all_to_all | solution.py:325
  48.5 11.0 %collective-permute-start = (bf16[3,64,2048]{2,1,0:T(8,128)(2,1)}, bf16[3,64,2048]{2,1,0:T(8,128)(2,1)S(1)}, u32[]{:S(2)}, u32[]{:S(2)}) collective-permute-start(bf16[3,64,2048]{2,1,0:T(8,128)(2,1)} %other_half.1), channel_id=1, source_target_pairs={{0,1},{1,0},{2,3},{3,2},{4,5},{5,4},{6,7},{7,6},{8,9},{9,8},{10,11... | collective-permute-start | bytes 2359304 | tf_op jit(solution)/shard_map/ppermute | solution.py:309
  59.5 21.7 %copy-start.2 = (bf16[3,64,2048]{2,1,0:T(8,128)(2,1)}, bf16[3,64,2048]{2,1,0:T(8,128)(2,1)S(1)}, u32[]{:S(2)}) copy-start(bf16[3,64,2048]{2,1,0:T(8,128)(2,1)S(1)} %collective-permute-done.wr_ref) | copy-start | bytes 2359300
  89.2 5.4 %collective-permute-start.1 = (f32[384,384]{1,0:T(8,128)}, f32[384,384]{1,0:T(8,128)S(1)}, u32[]{:S(2)}, u32[]{:S(2)}) collective-permute-start(f32[384,384]{1,0:T(8,128)} %forward.1.own_ref), channel_id=1, source_target_pairs={{0,1},{1,0},{2,3},{3,2},{4,5},{5,4},{6,7},{7,6},{8,9},{9,8},{10,11... | collective-permute-start | bytes 1769480 | tf_op jit(solution)/shard_map/ppermute | solution.py:309
  94.5 0.8 copy-start.5
  102.4 45.9 %all-to-all-start.2 = ((bf16[8,400,256]{2,1,0:T(8,128)(2,1)}), bf16[8,400,256]{2,1,0:T(8,128)(2,1)S(1)}, u32[]{:S(2)}, u32[]{:S(2)}) async-start(bf16[8,400,256]{2,1,0:T(8,128)(2,1)} %get-tuple-element.28), calls=%async_computation.2 | async-start | bytes 3276800 | tf_op jit(solution)/shard_map/all_to_all | solution.py:335
  113.0 48.9 %collective-permute-start.2 = (bf16[192,2048]{1,0:T(8,128)(2,1)}, bf16[192,2048]{1,0:T(8,128)(2,1)S(1)}, u32[]{:S(2)}, u32[]{:S(2)}) collective-permute-start(bf16[192,2048]{1,0:T(8,128)(2,1)} %partner_grads.1), channel_id=1, source_target_pairs={{0,1},{1,0},{2,3},{3,2},{4,5},{5,4},{6,7},{7,6},{8,9},{9,8},{10,11... | collective-permute-start | bytes 2359304 | tf_op jit(solution)/shard_map/ppermute | solution.py:309
  148.3 1.2 copy-start.1
  152.0 21.5 %all-to-all-start.3 = ((bf16[32,16,256]{2,1,0:T(8,128)(2,1)}), bf16[32,16,256]{2,1,0:T(8,128)(2,1)S(1)}, u32[]{:S(2)}, u32[]{:S(2)}) async-start(bf16[32,16,256]{2,1,0:T(8,128)(2,1)} %reduced.1), calls=%async_computation.3 | async-start | bytes 524288 | tf_op jit(solution)/shard_map/all_to_all | solution.py:336
  161.9 0.9 copy-start.4
  173.5 0.7 copy-start.3
Sparse Core Ops, SparseCore 0:
  37.1 44.0 all-gather.1

commit v2 on v1

v2 whole, which is shorter than its diff:
```python
import jax
import jax.numpy as jnp
from jax import lax
from jax.experimental import pallas as pl
from jax.experimental.pallas import tpu as pltpu
from jax.sharding import Mesh, PartitionSpec as P

TOK, TOP, EXPERTS, CAP = 128, 2, 32, 12
SLOTS = EXPERTS * CAP
ROWS = 2 * SLOTS
PAIR = 2 * CAP
WIDTH = 256
NY = 8
HALF = NY * WIDTH
HID = 64
EP = ("z", "x")
F32, BF16, I32 = jnp.float32, jnp.bfloat16, jnp.int32


def iota(shape, dim):
    return lax.broadcasted_iota(I32, shape, dim)


def slot_codes(rt):
    ids = iota((EXPERTS, TOK), 0)
    first, second = rt[0:1, :] == ids, rt[1:2, :] == ids
    hot = jnp.where(first, 1.0, 0.0) + jnp.where(second, 1.0, 0.0)
    upper = jnp.where(iota((TOK, TOK), 0) < iota((TOK, TOK), 1), 1.0, 0.0)
    rank = jnp.dot(hot.astype(BF16), upper.astype(BF16), preferred_element_type=F32)
    return jnp.where(hot > 0.5, rank, -1.0), first, second


def dispatch_kernel(rt_ref, gw_ref, tok_ref, cot_ref, out_ref):
    code, first, second = slot_codes(rt_ref[...])
    gw = gw_ref[...]
    weight = jnp.where(first, gw[0:1, :], 0.0) + jnp.where(second, gw[1:2, :], 0.0)
    shape = (EXPERTS, PAIR, TOK)
    code3 = jnp.broadcast_to(code[:, None, :], shape)
    weight3 = jnp.broadcast_to(weight[:, None, :], shape)
    at = iota(shape, 1)
    atf = at.astype(F32)
    sel_x = jnp.where(code3 == atf, jnp.where(at < CAP, 1.0, 0.0), 0.0)
    sel_g = jnp.where(code3 == atf - float(CAP), jnp.where(at >= CAP, 1.0, 0.0), 0.0)
    scale = jnp.sum(sel_g * weight3 + sel_x, axis=2, keepdims=True).reshape(ROWS, 1)
    select = jnp.concatenate(
        [sel_x.reshape(ROWS, TOK).astype(BF16), sel_g.reshape(ROWS, TOK).astype(BF16)], axis=1
    )
    source = jnp.concatenate([tok_ref[...], cot_ref[...]], axis=0)
    rows = jnp.dot(select, source, preferred_element_type=F32)
    out_ref[...] = (rows * scale).astype(BF16).reshape(EXPERTS, PAIR, WIDTH)


def dispatch(rt, gw, tokens, cotangent):
    out = (jax.ShapeDtypeStruct((EXPERTS, PAIR, WIDTH), BF16),)
    return kernel_call(dispatch_kernel, out, "dispatch", rt, gw, tokens, cotangent)[0]


def vmem(value):
    return pltpu.with_memory_space_constraint(value, pltpu.VMEM)


def kernel_call(body, out, name, *values, core=None, scratch=(), far=(), near=(), far_out=0):
    specs = [pl.BlockSpec(memory_space=pl.ANY)] * len(far)
    specs += [pl.BlockSpec(memory_space=pltpu.VMEM)] * len(near)
    specs += [pl.BlockSpec()] * len(values)
    values = [*far, *(vmem(v) for v in near), *values]
    if core is not None:
        specs, values = [pl.BlockSpec(memory_space=pltpu.SMEM)] + specs, [core] + values
    results = [
        pl.BlockSpec(memory_space=pl.ANY) if at < far_out else pl.BlockSpec()
        for at in range(len(out))
    ]
    return pl.pallas_call(
        body,
        in_specs=specs,
        out_specs=results,
        out_shape=list(out),
        scratch_shapes=list(scratch),
        name=name,
    )(*values)


def fetch(pairs, sems):
    copies = [
        pltpu.make_async_copy(there, here, sems.at[at]) for at, (there, here) in enumerate(pairs)
    ]
    for copy in copies:
        copy.start()
    return copies


def flags(count):
    return pltpu.SemaphoreType.DMA((count,))


def lanes_of(step, half):
    return pl.ds(pl.multiple_of((2 * step + half) * WIDTH, WIDTH), WIDTH)


def half_lanes(y):
    return slice(y * WIDTH, (y + 1) * WIDTH)


def split_kernel(c_ref, wg_ref, wu_ref, wd_ref, out_ref):
    for at, ref in enumerate((wg_ref, wu_ref, wd_ref)):
        for y in range(NY):
            out_ref[at, :, half_lanes(y)] = ref[:, lanes_of(y, 1 - c_ref[0])]


def other_half(core, wg, wu, wd):
    out = (jax.ShapeDtypeStruct((3, HID, HALF), BF16),)
    return kernel_call(split_kernel, out, "other_half", wg, wu, wd, core=core)[0]


def is_token_lane(shape):
    lane = iota(shape, 1)
    return lane - ((lane * 2731) >> 16) * PAIR < CAP


def forward_kernel(
    c_ref, xg_far, wg_far, wu_far, wd_far, wr_far, out_ref, xg_ref, wg_ref, wu_ref, wd_ref, wr_ref, sems
):
    weights = [(wg_far, wg_ref), (wd_far, wd_ref), (wu_far, wu_ref), (wr_far, wr_ref)]
    blocks = [(xg_far.at[y], xg_ref.at[y]) for y in range(NY)]
    copies = fetch(blocks[:1] + weights + blocks[1:], sems)
    for copy in copies[:5]:
        copy.wait()
    total = None
    for y in range(NY):
        if y > 0:
            copies[4 + y].wait()
        parts = []
        for at, ref in enumerate((wg_ref, wd_ref, wu_ref)):
            parts.append(ref[:, lanes_of(y, c_ref[0])])
            parts.append(wr_ref[(0, 2, 1)[at], :, half_lanes(y)])
        part = lax.dot_general(
            jnp.concatenate(parts, axis=0),
            xg_ref[y],
            (((1,), (1,)), ((), ())),
            preferred_element_type=F32,
        )
        total = part if total is None else total + part
    pair = 2 * HID
    out_ref[0:pair, :] = jnp.where(
        is_token_lane((pair, ROWS)), total[0:pair, :], total[pair : 2 * pair, :]
    )
    out_ref[pair : 2 * pair, :] = total[2 * pair : 3 * pair, :]


def forward(core, xg, wg, wu, wd, wr):
    out = (jax.ShapeDtypeStruct((4 * HID, ROWS), F32),)
    return kernel_call(
        forward_kernel,
        out,
        "forward",
        core=core,
        far=(xg, wg, wu, wd, wr),
        scratch=(
            pltpu.VMEM((NY, ROWS, WIDTH), BF16),
            pltpu.VMEM((HID, 2 * HALF), BF16),
            pltpu.VMEM((HID, 2 * HALF), BF16),
            pltpu.VMEM((HID, 2 * HALF), BF16),
            pltpu.VMEM((3, HID, HALF), BF16),
            flags(4 + NY),
        ),
    )[0]


def backward_kernel(
    c_ref, own_far, wg_far, wu_far, wr_far, got_ref, out_far, gate_ref, left_ref,
    own_ref, wg_ref, wu_ref, wr_ref, out_ref, sems, out_sems,
):
    copies = fetch(
        [
            (own_far, own_ref),
            (wg_far, wg_ref),
            (wu_far, wu_ref),
            (wr_far.at[0:2], wr_ref),
        ],
        sems,
    )
    copies[0].wait()

    def total(at):
        low, mid, high = 2 * at * HID, (2 * at + 1) * HID, (2 * at + 2) * HID
        return jnp.concatenate(
            [
                own_ref[low:mid, :] + got_ref[mid:high, :],
                own_ref[mid:high, :] + got_ref[low:mid, :],
            ],
            axis=0,
        )

    pre_gate, pre_up = total(0), total(1)
    keep = is_token_lane((2 * HID, ROWS))
    back = pltpu.roll(pre_gate, ROWS - CAP, 1)
    sig = 1.0 / (1.0 + jnp.exp(-jnp.where(keep, pre_gate, 0.0)))
    silu = pre_gate * sig
    hidden = jnp.where(keep, silu * pre_up, 0.0).astype(BF16).astype(F32)
    grad_gate = jnp.where(keep, back * pre_up * sig * (1.0 + pre_gate * (1.0 - sig)), 0.0)
    grad_up = jnp.where(keep, back * silu, 0.0)
    gate_ref[...] = jnp.broadcast_to(
        jnp.sum(hidden * back, axis=0, keepdims=True)[None], (NY, 1, ROWS)
    )
    shifted = pltpu.roll(hidden, CAP, 1)
    for at, grad in enumerate((grad_gate, grad_up, shifted)):
        grad = grad.astype(BF16)
        left_ref[0, at * HID : (at + 1) * HID, :] = grad[0:HID]
        left_ref[1, at * HID : (at + 1) * HID, :] = grad[HID : 2 * HID]
    both = jnp.concatenate([grad_gate.astype(BF16), grad_up.astype(BF16)], axis=0)
    slot = iota((SLOTS, ROWS), 0)
    lane = iota((SLOTS, ROWS), 1)
    compact = jnp.where(lane == slot + ((slot * 5462) >> 16) * CAP, 1.0, 0.0).astype(BF16)
    grads = lax.dot_general(
        compact, both, (((1,), (1,)), ((), ())), preferred_element_type=F32
    ).astype(BF16)
    for copy in copies[1:]:
        copy.wait()
    sent = []
    for y in range(NY):
        mats = jnp.concatenate(
            [
                wg_ref[:, lanes_of(y, c_ref[0])],
                wr_ref[0, :, half_lanes(y)],
                wu_ref[:, lanes_of(y, c_ref[0])],
                wr_ref[1, :, half_lanes(y)],
            ],
            axis=0,
        )
        out_ref[y] = jnp.dot(grads, mats, preferred_element_type=F32).astype(BF16)
        sent.append(pltpu.make_async_copy(out_ref.at[y], out_far.at[y], out_sems.at[y]))
        sent[y].start()
    for copy in sent:
        copy.wait()


def backward(core, own, got, wg, wu, wr):
    out = (
        jax.ShapeDtypeStruct((NY, SLOTS, WIDTH), BF16),
        jax.ShapeDtypeStruct((NY, 1, ROWS), F32),
        jax.ShapeDtypeStruct((2, 3 * HID, ROWS), BF16),
    )
    return kernel_call(
        backward_kernel,
        out,
        "backward",
        core=core,
        far=(own, wg, wu, wr),
        near=(got,),
        far_out=1,
        scratch=(
            pltpu.VMEM((4 * HID, ROWS), F32),
            pltpu.VMEM((HID, 2 * HALF), BF16),
            pltpu.VMEM((HID, 2 * HALF), BF16),
            pltpu.VMEM((2, HID, HALF), BF16),
            pltpu.VMEM((NY, SLOTS, WIDTH), BF16),
            flags(4),
            flags(NY),
        ),
    )


def partner_kernel(left_far, xg_far, out_ref, left_ref, xg_ref, sems):
    copies = fetch(
        [(left_far.at[1], left_ref)] + [(xg_far.at[y], xg_ref.at[y]) for y in range(NY)], sems
    )
    copies[0].wait()
    for y in range(NY):
        copies[1 + y].wait()
        out_ref[:, half_lanes(y)] = jnp.dot(
            left_ref[...], xg_ref[y], preferred_element_type=F32
        ).astype(BF16)


def partner_grads(left, xg):
    return kernel_call(
        partner_kernel,
        (jax.ShapeDtypeStruct((3 * HID, HALF), BF16),),
        "partner_grads",
        far=(left, xg),
        scratch=(
            pltpu.VMEM((3 * HID, ROWS), BF16),
            pltpu.VMEM((NY, ROWS, WIDTH), BF16),
            flags(1 + NY),
        ),
    )[0]


def merge_kernel(
    c_ref, left_far, xg_far, got_far, gate_far, up_far, down_far, left_ref, xg_ref, got_ref, out_ref, sems, out_sems
):
    copies = fetch(
        [(left_far.at[0], left_ref), (got_far, got_ref)]
        + [(xg_far.at[y], xg_ref.at[y]) for y in range(NY)],
        sems,
    )
    copies[0].wait()
    copies[1].wait()
    sent = []
    for y in range(NY):
        copies[2 + y].wait()
        mine = jnp.dot(left_ref[...], xg_ref[y], preferred_element_type=F32)
        theirs = got_ref[:, half_lanes(y)].astype(F32)
        both = slice(2 * y * WIDTH, (2 * y + 2) * WIDTH)
        for at, far in enumerate((gate_far, up_far, down_far)):
            rows = slice(at * HID, (at + 1) * HID)
            out_ref[at, :, lanes_of(y, c_ref[0])] = mine[rows, :]
            out_ref[at, :, lanes_of(y, 1 - c_ref[0])] = theirs[rows, :]
            sent.append(
                pltpu.make_async_copy(
                    out_ref.at[at, :, both], far.at[:, both], out_sems.at[3 * y + at]
                )
            )
            sent[-1].start()
    for copy in sent:
        copy.wait()


def merged_grads(core, left, xg, got):
    return kernel_call(
        merge_kernel,
        [jax.ShapeDtypeStruct((HID, 2 * HALF), F32)] * 3,
        "merged_grads",
        core=core,
        far=(left, xg, got),
        far_out=3,
        scratch=(
            pltpu.VMEM((3 * HID, ROWS), BF16),
            pltpu.VMEM((NY, ROWS, WIDTH), BF16),
            pltpu.VMEM((3 * HID, HALF), BF16),
            pltpu.VMEM((3, HID, 2 * HALF), F32),
            flags(2 + NY),
            flags(3 * NY),
        ),
    )


def reduce_kernel(got_ref, gate_ref, out_ref):
    total = got_ref[0].astype(F32)
    gate = gate_ref[0]
    for y in range(1, NY):
        total = total + got_ref[y].astype(F32)
        gate = gate + gate_ref[y]
    total = total.astype(BF16)
    src = iota((EXPERTS, ROWS), 0)
    lane = iota((EXPERTS, ROWS), 1)
    table = jnp.where(
        (lane * 2731) >> 16 == src, jnp.broadcast_to(gate, (EXPERTS, ROWS)), 0.0
    ).astype(BF16)
    at = iota((ROWS, WIDTH), 0)
    picks = jnp.where(
        at - ((at * 2731) >> 16) * PAIR == iota((ROWS, WIDTH), 1), 1.0, 0.0
    ).astype(BF16)
    shares = jnp.dot(table, picks, preferred_element_type=F32).astype(BF16)
    row = iota((EXPERTS * 16, SLOTS + EXPERTS), 0)
    col = iota((EXPERTS * 16, SLOTS + EXPERTS), 1)
    source = row >> 4
    want = jnp.where(
        row - source * 16 < CAP,
        source * CAP + row - source * 16,
        jnp.where(row - source * 16 == CAP, SLOTS + source, -1),
    )
    place = jnp.where(col == want, 1.0, 0.0).astype(BF16)
    rows = jnp.dot(
        place, jnp.concatenate([total, shares], axis=0), preferred_element_type=F32
    )
    out_ref[...] = rows.astype(BF16).reshape(EXPERTS, 16, WIDTH)


def reduced(got, gate):
    return kernel_call(
        reduce_kernel,
        (jax.ShapeDtypeStruct((EXPERTS, 16, WIDTH), BF16),),
        "reduced",
        gate,
        near=(got,),
    )[0]


def combine_kernel(back_ref, rt_ref, gw_ref, out_ref, gate_ref):
    code, first, second = slot_codes(rt_ref[...])
    shape = (EXPERTS, 16, TOK)
    code3 = jnp.broadcast_to(code[:, None, :], shape)
    select = jnp.where(code3 == iota(shape, 1).astype(F32), 1.0, 0.0)
    select = select.reshape(EXPERTS * 16, TOK).T.astype(BF16)
    back = back_ref[...]
    rows = jnp.dot(
        select, back.reshape(EXPERTS * 16, WIDTH), preferred_element_type=F32
    )
    out_ref[...] = rows.astype(BF16)
    shares = back[:, CAP, 0:TOK].astype(F32)
    mine = jnp.zeros((EXPERTS, TOK), F32)
    for p in range(CAP):
        mine = mine + jnp.where(code == float(p), shares[:, p : p + 1], 0.0)
    top = jnp.sum(jnp.where(first, mine, 0.0), axis=0, keepdims=True)
    low = jnp.sum(jnp.where(second, mine, 0.0), axis=0, keepdims=True)
    gate_ref[...] = jnp.concatenate([top, low], axis=0) / gw_ref[...]


def combine(rt, gw, back):
    out = (
        jax.ShapeDtypeStruct((TOK, WIDTH), BF16),
        jax.ShapeDtypeStruct((TOP, TOK), F32),
    )
    return kernel_call(combine_kernel, out, "combine", rt, gw, near=(back,))


def core_swap(value):
    return lax.ppermute(value, "c", [(0, 1), (1, 0)])


def shards(tokens, cotangent, routes, gate_weight, w_gate, w_up, w_down, shared_hidden):
    rt, gw = routes.T, gate_weight.T
    core = lax.axis_index("c").astype(I32).reshape(1)
    wg, wu, wd = w_gate[0], w_up[0], w_down[0]
    sent = dispatch(rt, gw, tokens, cotangent)
    rows = lax.all_to_all(sent, EP, split_axis=0, concat_axis=0, tiled=True)
    rows, cotangent, wg, wu, wd = lax.optimization_barrier((rows, cotangent, wg, wu, wd))
    xg = lax.all_gather(rows.reshape(ROWS, WIDTH), "y", axis=0, tiled=False)

    wr = core_swap(other_half(core, wg, wu, wd))
    shared = lax.dot_general(
        shared_hidden, cotangent, (((0,), (0,)), ((), ())), preferred_element_type=F32
    ).astype(BF16)
    shared = lax.all_to_all(
        shared.reshape(EXPERTS, -1, WIDTH), EP, split_axis=0, concat_axis=0, tiled=True
    )
    shared_grad = jnp.sum(shared.astype(F32), axis=0)
    xg, wr, shared_grad = lax.optimization_barrier((xg, wr, shared_grad))

    own = forward(core, xg, wg, wu, wd, wr)
    parts, gate, left = backward(core, own, core_swap(own), wg, wu, wr)
    got = lax.all_to_all(parts, "y", split_axis=0, concat_axis=0, tiled=True)
    theirs = partner_grads(left, xg)
    theirs, gate = lax.optimization_barrier((theirs, gate))
    theirs = core_swap(theirs)
    gate = lax.all_to_all(gate, "y", split_axis=0, concat_axis=0, tiled=True)
    grads = merged_grads(core, left, xg, theirs)
    back = lax.all_to_all(reduced(got, gate), EP, split_axis=0, concat_axis=0, tiled=True)
    tokens_grad, gate_grad = combine(rt, gw, back)
    return (tokens_grad, gate_grad.T, grads[0][None], grads[1][None], grads[2][None], shared_grad)


def solution(mesh):
    split = Mesh(mesh.devices.reshape(8, 4, 8, 2), ("z", "x", "y", "c"))
    ep, tp = ("z", "x"), ("y", "c")
    placed = (
        P(ep, tp),
        P(ep, tp),
        P(ep, None),
        P(ep, None),
        P(ep, tp, None),
        P(ep, tp, None),
        P(ep, tp, None),
        P(ep, None),
    )
    return jax.shard_map(
        shards,
        mesh=split,
        in_specs=placed,
        out_specs=(
            P(ep, tp),
            P(ep, None),
            P(ep, tp, None),
            P(ep, tp, None),
            P(ep, tp, None),
            P(ep, tp),
        ),
        check_vma=False,
    )
```

time: 184 us -> 189 us (1.027)
  Pallas kernels: 40.3 us -> 27.2 us
  blocking collectives: 27.6 us -> 38.3 us
  waiting for transfers between devices: 66.6 us -> 75.8 us
  local copies, waits for them, and re-layouts: 4.61 us -> 1.91 us
    pallas_call x8, Pallas kernels: 40.3 us -> 27.2 us  [kernel_call(): pl.pallas_call(body, in_specs=specs, out_specs=results, out_shape=list(ou...]
    all_to_all x0 -> x1, blocking collectives: none -> 10.6 us  [shards(): gate = lax.all_to_all(gate, 'y', split_axis=0, concat_axis=0, tiled=True)]
    all_to_all x1, waiting for transfers between devices: 32.7 us -> 36.7 us  [shards(): got = lax.all_to_all(parts, 'y', split_axis=0, concat_axis=0, tiled=True)]
    all_to_all x1, waiting for transfers between devices: 6.7 us -> 9.48 us  [shards(): lax.all_to_all(shared.reshape(EXPERTS, -1, WIDTH), EP, split_axis=0, conc...]
    unnamed x14 -> x12, local copies, waits for them, and re-layouts: 3.61 us -> 0.91 us
    all_to_all x1, waiting for transfers between devices: 3.59 us -> 5.78 us  [shards(): lax.all_to_all(reduced(got, gate), EP, split_axis=0, concat_axis=0, tiled...]
  transfers between devices with their start and end apart: 7 -> 7, of which waited for: 5 -> 5; matrix products, arithmetic and copies ran while one was open for 1% -> 1% of each run, Pallas kernels for 12% -> 5%
where the time goes in v2:
time: 189 us; the launch traced here: 188 us
  waiting for transfers between devices  75.8 us (40%)
  blocking collectives  38.3 us (20%)
  starting transfers between devices  29.5 us (16%)
  Pallas kernels  27.2 us (14%)
  between operations  14.2 us (8%)
  local copies, waits for them, and re-layouts  1.91 us (1%)
    all_to_all x1, waiting for transfers between devices, shards(): got = lax.all_to_all(parts, 'y', split_axis=0, concat_axis=0, tiled=True)  36.7 us
    all_to_all x1, blocking collectives, shards(): rows = lax.all_to_all(sent, EP, split_axis=0, concat_axis=0, tiled=True)  27.6 us
    pallas_call x8, Pallas kernels, kernel_call(): pl.pallas_call(body, in_specs=specs, out_specs=results, out_shape=list(ou...  27.2 us
    all_gather x1, waiting for transfers between devices, shards(): xg = lax.all_gather(rows.reshape(ROWS, WIDTH), 'y', axis=0, tiled=False)  21.7 us
    ppermute x3, starting transfers between devices, core_swap(): return lax.ppermute(value, 'c', [(0, 1), (1, 0)])  10.8 us
    all_to_all x1, blocking collectives, shards(): gate = lax.all_to_all(gate, 'y', split_axis=0, concat_axis=0, tiled=True)  10.6 us
    all_to_all x1, starting transfers between devices, shards(): lax.all_to_all(reduced(got, gate), EP, split_axis=0, concat_axis=0, tiled...  9.89 us
    all_to_all x1, waiting for transfers between devices, shards(): lax.all_to_all(shared.reshape(EXPERTS, -1, WIDTH), EP, split_axis=0, conc...  9.48 us
  transfers between devices with their start and end apart: 7, of which 5 were waited for; matrix products, arithmetic and copies ran while one was open for 1% of the time, Pallas kernels for 5%

profile of v2, /device:TPU:1, one launch (start us, length us, event | category | flops | bytes accessed | tf_op | source)
XLA Modules:
  0.0 187.9 jit_solution(7048667385020370814)
XLA Ops:
  7.2 0.0 copy-start
  7.2 0.0 copy-start.4
  7.2 0.0 all-gather.2.cloned.1.call-start
  7.2 2.1 %dispatch.1 = bf16[32,24,256]{2,1,0:T(8,128)(2,1)} custom-call(s32[2,128]{1,0:T(2,128)} %bitcast.25, f32[2,128]{1,0:T(2,128)} %bitcast.27, bf16[128,256]{1,0:T(8,128)(2,1)} %tok_ref.1, bf16[128,256]{1,0:T(8,128)(2,1)} %cot_ref.1), custom_call_target="tpu_custom_call" | custom-call | tf_op jit(solution)/shard_map/dispatch/pallas_call | solution.py:73
  9.3 27.6 %all_to_all.25 = bf16[32,24,256]{2,1,0:T(8,128)(2,1)} all-to-all(bf16[32,24,256]{2,1,0:T(8,128)(2,1)} %dispatch.1), channel_id=1, replica_groups=mesh['z'=8,'x'=4,'y'=8,'c'=2] {'z','x'}, dimensions={0} | all-to-all | bytes 786432 | tf_op jit(solution)/shard_map/all_to_all | solution.py:417
  37.0 0.0 all-gather.2.cloned.1.call-update
  37.0 0.0 copy-done
  37.0 0.0 copy-done.4
  37.0 0.3 fusion
  37.3 1.0 copy.15
  38.3 5.0 %all-to-all-start.1 = ((bf16[32,32,256]{2,1,0:T(8,128)(2,1)}), bf16[32,32,256]{2,1,0:T(8,128)(2,1)S(1)}, u32[]{:S(2)}, u32[]{:S(2)}) async-start(bf16[32,32,256]{2,1,0:T(8,128)(2,1)} %bitcast.8), calls=%async_computation.1 | async-start | bytes 1048576 | tf_op jit(solution)/shard_map/all_to_all | solution.py:425
  43.4 2.3 %other_half.1 = bf16[3,64,2048]{2,1,0:T(8,128)(2,1)} custom-call(s32[1]{0:T(128)} %bitcast.c_ref, bf16[64,4096]{1,0:T(8,128)(2,1)} %bitcast.16, bf16[64,4096]{1,0:T(8,128)(2,1)} %bitcast.19, bf16[64,4096]{1,0:T(8,128)(2,1)} %bitcast.22), custom_call_target="tpu_custom_call" | custom-call | tf_op jit(solution)/shard_map/other_half/pallas_call | solution.py:73
  45.7 3.6 %collective-permute-start = (bf16[3,64,2048]{2,1,0:T(8,128)(2,1)}, bf16[3,64,2048]{2,1,0:T(8,128)(2,1)S(1)}, u32[]{:S(2)}, u32[]{:S(2)}) collective-permute-start(bf16[3,64,2048]{2,1,0:T(8,128)(2,1)} %other_half.1), channel_id=1, source_target_pairs={{0,1},{1,0},{2,3},{3,2},{4,5},{5,4},{6,7},{7,6},{8,9},{9,8},{10,11... | collective-permute-start | bytes 2359304 | tf_op jit(solution)/shard_map/ppermute | solution.py:409
  49.3 9.5 %all-to-all-done.1 = bf16[32,32,256]{2,1,0:T(8,128)(2,1)S(1)} async-done(((bf16[32,32,256]{2,1,0:T(8,128)(2,1)}), bf16[32,32,256]{2,1,0:T(8,128)(2,1)S(1)}, u32[]{:S(2)}, u32[]{:S(2)}) %all-to-all-start.1) | async-done | bytes 524320 | tf_op jit(solution)/shard_map/all_to_all | solution.py:425
  58.8 0.7 convert_reduce_fusion
  59.5 0.0 collective-permute-done.wr_far
  59.5 0.0 copy-start.1
  59.5 21.7 %all-gather.2.cloned.1.call-done.xg_far = bf16[8,768,256]{2,1,0:T(8,128)(2,1)} async-done(((bf16[1,768,256]{2,1,0:T(8,128)(2,1)}), bf16[8,768,256]{2,1,0:T(8,128)(2,1)}) %all-gather.2.cloned.1.call-update) | async-done | bytes 3145744 | tf_op jit(solution)/shard_map/all_gather | solution.py:419
  81.2 0.0 copy-done.1
  81.2 5.4 %forward.1.own_far = f32[256,768]{1,0:T(8,128)} custom-call(s32[1]{0:T(128)} %bitcast.c_ref, bf16[8,768,256]{2,1,0:T(8,128)(2,1)} %all-gather.2.cloned.1.call-done.xg_far, bf16[64,4096]{1,0:T(8,128)(2,1)} %bitcast.17, bf16[64,4096]{1,0:T(8,128)(2,1)} %bitcast.20, bf16[64,4096]{1,0:T(8,128)(2,1)} %bitcast.23, bf16[3,64,2048]{2,1,0:T(8,128)(2,1)} %copy-done.1), custom_call_target="tpu_custom_call" | custom-call | tf_op jit(solution)/shard_map/forward/pallas_call | solution.py:73
  86.6 3.6 %collective-permute-start.1 = (f32[256,768]{1,0:T(8,128)}, f32[256,768]{1,0:T(8,128)S(1)}, u32[]{:S(2)}, u32[]{:S(2)}) collective-permute-start(f32[256,768]{1,0:T(8,128)} %forward.1.own_far), channel_id=1, source_target_pairs={{0,1},{1,0},{2,3},{3,2},{4,5},{5,4},{6,7},{7,6},{8,9},{9,8},{10,11... | collective-permute-start | bytes 2359304 | tf_op jit(solution)/shard_map/ppermute | solution.py:409
  90.2 2.1 %collective-permute-done.1.got_ref = f32[256,768]{1,0:T(8,128)S(1)} collective-permute-done((f32[256,768]{1,0:T(8,128)}, f32[256,768]{1,0:T(8,128)S(1)}, u32[]{:S(2)}, u32[]{:S(2)}) %collective-permute-start.1) | collective-permute-done | bytes 786464 | tf_op jit(solution)/shard_map/ppermute | solution.py:409
  92.3 4.3 %backward.1 = (bf16[8,384,256]{2,1,0:T(8,128)(2,1)}, f32[8,1,768]{2,1,0:T(1,128)}, bf16[2,192,768]{2,1,0:T(8,128)(2,1)}) custom-call(s32[1]{0:T(128)} %bitcast.c_ref, f32[256,768]{1,0:T(8,128)} %forward.1.own_far, bf16[64,4096]{1,0:T(8,128)(2,1)} %bitcast.18, bf16[64,4096]{1,0:T(8,128)(2,1)} %bitcast.21, bf16[3,64,2048]{2,1,0:T(8,128)(2,1)} %copy-done.1, ...), custom_call_target="tpu_custom_call" | custom-call | tf_op jit(solution)/shard_map/backward/pallas_call | solution.py:73
  96.6 0.0 copy-start.5
  96.7 4.5 %partner_grads.1 = bf16[192,2048]{1,0:T(8,128)(2,1)} custom-call(bf16[2,192,768]{2,1,0:T(8,128)(2,1)} %get-tuple-element.32.left_far, bf16[8,768,256]{2,1,0:T(8,128)(2,1)} %all-gather.2.cloned.1.call-done.xg_far), custom_call_target="tpu_custom_call" | custom-call | tf_op jit(solution)/shard_map/partner_grads/pallas_call | solution.py:73
  101.1 0.0 copy-done.5
  101.1 10.6 %all_to_all.26.gate_ref = f32[8,1,768]{2,1,0:T(1,128)} all-to-all(f32[8,1,768]{2,1,0:T(1,128)S(1)} %copy-done.5), channel_id=1, replica_groups=mesh['z'=8,'x'=4,'y'=8,'c'=2] {'y'}, dimensions={0} | all-to-all | bytes 49152 | tf_op jit(solution)/shard_map/all_to_all | solution.py:437
  111.8 0.0 copy-start.3
  111.8 3.7 %all-to-all-start.2 = ((bf16[8,384,256]{2,1,0:T(8,128)(2,1)}), bf16[8,384,256]{2,1,0:T(8,128)(2,1)S(1)}, u32[]{:S(2)}, u32[]{:S(2)}) async-start(bf16[8,384,256]{2,1,0:T(8,128)(2,1)} %get-tuple-element.31), calls=%async_computation.2 | async-start | bytes 3145728 | tf_op jit(solution)/shard_map/all_to_all | solution.py:433
  115.5 0.0 copy-done.3
  115.5 3.7 %collective-permute-start.2 = (bf16[192,2048]{1,0:T(8,128)(2,1)S(1)}, bf16[192,2048]{1,0:T(8,128)(2,1)S(1)}, u32[]{:S(2)}, u32[]{:S(2)}) collective-permute-start(bf16[192,2048]{1,0:T(8,128)(2,1)S(1)} %copy-done.3), channel_id=1, source_target_pairs={{0,1},{1,0},{2,3},{3,2},{4,5},{5,4},{6,7},{7,6},{8,9},{9,8},{10,11... | collective-permute-start | bytes 2359304 | tf_op jit(solution)/shard_map/ppermute | solution.py:409
  119.2 36.7 %all-to-all-done.2.got_ref = bf16[8,384,256]{2,1,0:T(8,128)(2,1)S(1)} async-done(((bf16[8,384,256]{2,1,0:T(8,128)(2,1)}), bf16[8,384,256]{2,1,0:T(8,128)(2,1)S(1)}, u32[]{:S(2)}, u32[]{:S(2)}) %all-to-all-start.2) | async-done | bytes 1572896 | tf_op jit(solution)/shard_map/all_to_all | solution.py:433
  155.9 2.1 %reduced.1 = bf16[32,16,256]{2,1,0:T(8,128)(2,1)} custom-call(bf16[8,384,256]{2,1,0:T(8,128)(2,1)S(1)} %all-to-all-done.2.got_ref, f32[8,1,768]{2,1,0:T(1,128)} %all_to_all.26.gate_ref), custom_call_target="tpu_custom_call" | custom-call | tf_op jit(solution)/shard_map/reduced/pallas_call | solution.py:73
  158.0 9.9 %all-to-all-start.4 = ((bf16[32,16,256]{2,1,0:T(8,128)(2,1)}), bf16[32,16,256]{2,1,0:T(8,128)(2,1)S(1)}, u32[]{:S(2)}, u32[]{:S(2)}) async-start(bf16[32,16,256]{2,1,0:T(8,128)(2,1)} %reduced.1), calls=%async_computation.4 | async-start | bytes 524288 | tf_op jit(solution)/shard_map/all_to_all | solution.py:439
  167.9 0.0 collective-permute-done.2.got_far
  167.9 0.0 copy-start.2
  167.9 0.9 copy-done.2
  168.8 4.8 %merged_grads.1 = (f32[64,4096]{1,0:T(8,128)}, f32[64,4096]{1,0:T(8,128)}, f32[64,4096]{1,0:T(8,128)}) custom-call(s32[1]{0:T(128)} %bitcast.c_ref, bf16[2,192,768]{2,1,0:T(8,128)(2,1)} %get-tuple-element.32.left_far, bf16[8,768,256]{2,1,0:T(8,128)(2,1)} %all-gather.2.cloned.1.call-done.xg_far, bf16[192,2048]{1,0:T(8,128)(2,1)} %copy-done.2), custom_call_target="tpu_custom_call" | custom-call | tf_op jit(solution)/shard_map/merged_grads/pallas_call | solution.py:73
  173.6 5.8 %all-to-all-done.4.back_ref = bf16[32,16,256]{2,1,0:T(8,128)(2,1)S(1)} async-done(((bf16[32,16,256]{2,1,0:T(8,128)(2,1)}), bf16[32,16,256]{2,1,0:T(8,128)(2,1)S(1)}, u32[]{:S(2)}, u32[]{:S(2)}) %all-to-all-start.4) | async-done | bytes 262176 | tf_op jit(solution)/shard_map/all_to_all | solution.py:439
  179.3 1.7 combine.1
Async XLA Ops:
  7.2 29.8 %copy-start = (bf16[128,1024]{1,0:T(8,128)(2,1)S(1)}, bf16[128,1024]{1,0:T(8,128)(2,1)}, u32[]{:S(2)}) copy-start(bf16[128,1024]{1,0:T(8,128)(2,1)} %param.15) | copy-start | bytes 786436
  7.2 29.8 %copy-start.4 = (bf16[128,256]{1,0:T(8,128)(2,1)S(1)}, bf16[128,256]{1,0:T(8,128)(2,1)}, u32[]{:S(2)}) copy-start(bf16[128,256]{1,0:T(8,128)(2,1)} %cot_ref.1) | copy-start | bytes 196612
  7.2 74.0 %all-gather.2.cloned.1.call-start = ((), (), s32[]{:S(2)}) async-start(), calls=%async_computation.5 | async-start | bytes 3538944 | tf_op jit(solution)/shard_map/all_gather | solution.py:419
  38.3 20.5 %all-to-all-start.1 = ((bf16[32,32,256]{2,1,0:T(8,128)(2,1)}), bf16[32,32,256]{2,1,0:T(8,128)(2,1)S(1)}, u32[]{:S(2)}, u32[]{:S(2)}) async-start(bf16[32,32,256]{2,1,0:T(8,128)(2,1)} %bitcast.8), calls=%async_computation.1 | async-start | bytes 1048576 | tf_op jit(solution)/shard_map/all_to_all | solution.py:425
  45.7 13.8 %collective-permute-start = (bf16[3,64,2048]{2,1,0:T(8,128)(2,1)}, bf16[3,64,2048]{2,1,0:T(8,128)(2,1)S(1)}, u32[]{:S(2)}, u32[]{:S(2)}) collective-permute-start(bf16[3,64,2048]{2,1,0:T(8,128)(2,1)} %other_half.1), channel_id=1, source_target_pairs={{0,1},{1,0},{2,3},{3,2},{4,5},{5,4},{6,7},{7,6},{8,9},{9,8},{10,11... | collective-permute-start | bytes 2359304 | tf_op jit(solution)/shard_map/ppermute | solution.py:409
  59.5 21.7 %copy-start.1 = (bf16[3,64,2048]{2,1,0:T(8,128)(2,1)}, bf16[3,64,2048]{2,1,0:T(8,128)(2,1)S(1)}, u32[]{:S(2)}) copy-start(bf16[3,64,2048]{2,1,0:T(8,128)(2,1)S(1)} %collective-permute-done.wr_far) | copy-start | bytes 2359300
  86.6 5.7 %collective-permute-start.1 = (f32[256,768]{1,0:T(8,128)}, f32[256,768]{1,0:T(8,128)S(1)}, u32[]{:S(2)}, u32[]{:S(2)}) collective-permute-start(f32[256,768]{1,0:T(8,128)} %forward.1.own_far), channel_id=1, source_target_pairs={{0,1},{1,0},{2,3},{3,2},{4,5},{5,4},{6,7},{7,6},{8,9},{9,8},{10,11... | collective-permute-start | bytes 2359304 | tf_op jit(solution)/shard_map/ppermute | solution.py:409
  96.6 4.5 %copy-start.5 = (f32[8,1,768]{2,1,0:T(1,128)S(1)}, f32[8,1,768]{2,1,0:T(1,128)}, u32[]{:S(2)}) copy-start(f32[8,1,768]{2,1,0:T(1,128)} %get-tuple-element.34) | copy-start | bytes 73732
  111.8 3.7 %copy-start.3 = (bf16[192,2048]{1,0:T(8,128)(2,1)S(1)}, bf16[192,2048]{1,0:T(8,128)(2,1)}, u32[]{:S(2)}) copy-start(bf16[192,2048]{1,0:T(8,128)(2,1)} %partner_grads.1) | copy-start | bytes 2359300
  111.8 44.1 %all-to-all-start.2 = ((bf16[8,384,256]{2,1,0:T(8,128)(2,1)}), bf16[8,384,256]{2,1,0:T(8,128)(2,1)S(1)}, u32[]{:S(2)}, u32[]{:S(2)}) async-start(bf16[8,384,256]{2,1,0:T(8,128)(2,1)} %get-tuple-element.31), calls=%async_computation.2 | async-start | bytes 3145728 | tf_op jit(solution)/shard_map/all_to_all | solution.py:433
  115.5 52.4 %collective-permute-start.2 = (bf16[192,2048]{1,0:T(8,128)(2,1)S(1)}, bf16[192,2048]{1,0:T(8,128)(2,1)S(1)}, u32[]{:S(2)}, u32[]{:S(2)}) collective-permute-start(bf16[192,2048]{1,0:T(8,128)(2,1)S(1)} %copy-done.3), channel_id=1, source_target_pairs={{0,1},{1,0},{2,3},{3,2},{4,5},{5,4},{6,7},{7,6},{8,9},{9,8},{10,11... | collective-permute-start | bytes 2359304 | tf_op jit(solution)/shard_map/ppermute | solution.py:409
  158.0 21.4 %all-to-all-start.4 = ((bf16[32,16,256]{2,1,0:T(8,128)(2,1)}), bf16[32,16,256]{2,1,0:T(8,128)(2,1)S(1)}, u32[]{:S(2)}, u32[]{:S(2)}) async-start(bf16[32,16,256]{2,1,0:T(8,128)(2,1)} %reduced.1), calls=%async_computation.4 | async-start | bytes 524288 | tf_op jit(solution)/shard_map/all_to_all | solution.py:439
  167.9 0.9 copy-start.2
Sparse Core Ops, SparseCore 0:
  37.1 44.0 all-gather.1

commit v3 on v2

--- a/solution.py
+++ b/solution.py
@@ -13,6 +13,7 @@
 NY = 8
 HALF = NY * WIDTH
 HID = 64
+BACK = SLOTS + 8
 EP = ("z", "x")
 F32, BF16, I32 = jnp.float32, jnp.bfloat16, jnp.int32
 
@@ -51,7 +52,7 @@
 
 
 def dispatch(rt, gw, tokens, cotangent):
-    out = (jax.ShapeDtypeStruct((EXPERTS, PAIR, WIDTH), BF16),)
+    out = (pltpu.VMEM((EXPERTS, PAIR, WIDTH), BF16),)
     return kernel_call(dispatch_kernel, out, "dispatch", rt, gw, tokens, cotangent)[0]
 
 
@@ -67,8 +68,12 @@
     if core is not None:
         specs, values = [pl.BlockSpec(memory_space=pltpu.SMEM)] + specs, [core] + values
     results = [
-        pl.BlockSpec(memory_space=pl.ANY) if at < far_out else pl.BlockSpec()
-        for at in range(len(out))
+        pl.BlockSpec(memory_space=pl.ANY)
+        if at < far_out
+        else pl.BlockSpec()
+        if isinstance(shape, jax.ShapeDtypeStruct)
+        else pl.BlockSpec(memory_space=pltpu.VMEM)
+        for at, shape in enumerate(out)
     ]
     return pl.pallas_call(
         body,
@@ -167,7 +172,7 @@
 
 
 def backward_kernel(
-    c_ref, own_far, wg_far, wu_far, wr_far, got_ref, out_far, gate_ref, left_ref,
+    c_ref, own_far, wg_far, wu_far, wr_far, got_ref, out_far, left_ref,
     own_ref, wg_ref, wu_ref, wr_ref, out_ref, sems, out_sems,
 ):
     copies = fetch(
@@ -199,9 +204,10 @@
     hidden = jnp.where(keep, silu * pre_up, 0.0).astype(BF16).astype(F32)
     grad_gate = jnp.where(keep, back * pre_up * sig * (1.0 + pre_gate * (1.0 - sig)), 0.0)
     grad_up = jnp.where(keep, back * silu, 0.0)
-    gate_ref[...] = jnp.broadcast_to(
-        jnp.sum(hidden * back, axis=0, keepdims=True)[None], (NY, 1, ROWS)
-    )
+    gate = jnp.sum(hidden * back, axis=0, keepdims=True)
+    upper = gate.astype(BF16).astype(F32)
+    tail = [part[:, half_lanes(at)] for part in (upper, gate - upper) for at in range(3)]
+    tail = jnp.concatenate(tail + [jnp.zeros((2, WIDTH), F32)], axis=0).astype(BF16)
     shifted = pltpu.roll(hidden, CAP, 1)
     for at, grad in enumerate((grad_gate, grad_up, shifted)):
         grad = grad.astype(BF16)
@@ -227,7 +233,8 @@
             ],
             axis=0,
         )
-        out_ref[y] = jnp.dot(grads, mats, preferred_element_type=F32).astype(BF16)
+        out_ref[y, 0:SLOTS, :] = jnp.dot(grads, mats, preferred_element_type=F32).astype(BF16)
+        out_ref[y, SLOTS:BACK, :] = tail
         sent.append(pltpu.make_async_copy(out_ref.at[y], out_far.at[y], out_sems.at[y]))
         sent[y].start()
     for copy in sent:
@@ -236,8 +243,7 @@
 
 def backward(core, own, got, wg, wu, wr):
     out = (
-        jax.ShapeDtypeStruct((NY, SLOTS, WIDTH), BF16),
-        jax.ShapeDtypeStruct((NY, 1, ROWS), F32),
+        jax.ShapeDtypeStruct((NY, BACK, WIDTH), BF16),
         jax.ShapeDtypeStruct((2, 3 * HID, ROWS), BF16),
     )
     return kernel_call(
@@ -253,7 +259,7 @@
             pltpu.VMEM((HID, 2 * HALF), BF16),
             pltpu.VMEM((HID, 2 * HALF), BF16),
             pltpu.VMEM((2, HID, HALF), BF16),
-            pltpu.VMEM((NY, SLOTS, WIDTH), BF16),
+            pltpu.VMEM((NY, BACK, WIDTH), BF16),
             flags(4),
             flags(NY),
         ),
@@ -335,13 +341,11 @@
     )
 
 
-def reduce_kernel(got_ref, gate_ref, out_ref):
-    total = got_ref[0].astype(F32)
-    gate = gate_ref[0]
-    for y in range(1, NY):
-        total = total + got_ref[y].astype(F32)
-        gate = gate + gate_ref[y]
-    total = total.astype(BF16)
+def place_kernel(got_ref, out_ref):
+    total = got_ref[...].astype(F32)
+    gate = total[SLOTS : SLOTS + 3, :] + total[SLOTS + 3 : SLOTS + 6, :]
+    gate = jnp.concatenate([gate[at : at + 1, :] for at in range(3)], axis=1)
+    total = total[0:SLOTS, :].astype(BF16)
     src = iota((EXPERTS, ROWS), 0)
     lane = iota((EXPERTS, ROWS), 1)
     table = jnp.where(
@@ -367,14 +371,9 @@
     out_ref[...] = rows.astype(BF16).reshape(EXPERTS, 16, WIDTH)
 
 
-def reduced(got, gate):
-    return kernel_call(
-        reduce_kernel,
-        (jax.ShapeDtypeStruct((EXPERTS, 16, WIDTH), BF16),),
-        "reduced",
-        gate,
-        near=(got,),
-    )[0]
+def placed_rows(got):
+    out = (pltpu.VMEM((EXPERTS, 16, WIDTH), BF16),)
+    return kernel_call(place_kernel, out, "placed_rows", got)[0]
 
 
 def combine_kernel(back_ref, rt_ref, gw_ref, out_ref, gate_ref):
@@ -429,14 +428,12 @@
     xg, wr, shared_grad = lax.optimization_barrier((xg, wr, shared_grad))
 
     own = forward(core, xg, wg, wu, wd, wr)
-    parts, gate, left = backward(core, own, core_swap(own), wg, wu, wr)
-    got = lax.all_to_all(parts, "y", split_axis=0, concat_axis=0, tiled=True)
-    theirs = partner_grads(left, xg)
-    theirs, gate = lax.optimization_barrier((theirs, gate))
-    theirs = core_swap(theirs)
-    gate = lax.all_to_all(gate, "y", split_axis=0, concat_axis=0, tiled=True)
+    parts, left = backward(core, own, core_swap(own), wg, wu, wr)
+    got = lax.psum_scatter(parts, "y", scatter_dimension=0, tiled=False)
+    theirs = core_swap(partner_grads(left, xg))
     grads = merged_grads(core, left, xg, theirs)
-    back = lax.all_to_all(reduced(got, gate), EP, split_axis=0, concat_axis=0, tiled=True)
+    got, *grads = lax.optimization_barrier((got, *grads))
+    back = lax.all_to_all(placed_rows(got), EP, split_axis=0, concat_axis=0, tiled=True)
     tokens_grad, gate_grad = combine(rt, gw, back)
     return (tokens_grad, gate_grad.T, grads[0][None], grads[1][None], grads[2][None], shared_grad)
 

time: 189 us -> 168 us (0.89)
  the two profiles are of different devices: /device:TPU:1 before, /device:TPU:24 now
where the time goes in v3:
time: 168 us
  waiting for transfers between devices  64 us (38%)
  blocking collectives  49.8 us (30%)
  Pallas kernels  25.8 us (15%)
  between operations  14.1 us (8%)
  starting transfers between devices  10.2 us (6%)
  local copies, waits for them, and re-layouts  1.92 us (1%)
    all_to_all x1, blocking collectives, shards(): rows = lax.all_to_all(sent, EP, split_axis=0, concat_axis=0, tiled=True)  28.4 us
    reduce_scatter x1, waiting for transfers between devices, shards(): got = lax.psum_scatter(parts, 'y', scatter_dimension=0, tiled=False)  27.9 us
    pallas_call x8, Pallas kernels, kernel_call(): pl.pallas_call(body, in_specs=specs, out_specs=results, out_shape=list(ou...  25.8 us
    all_to_all x1, blocking collectives, shards(): lax.all_to_all(placed_rows(got), EP, split_axis=0, concat_axis=0, tiled=T...  21.4 us
    all_gather x1, waiting for transfers between devices, shards(): xg = lax.all_gather(rows.reshape(ROWS, WIDTH), 'y', axis=0, tiled=False)  18.4 us
    all_to_all x1, waiting for transfers between devices, shards(): lax.all_to_all(shared.reshape(EXPERTS, -1, WIDTH), EP, split_axis=0, conc...  12.8 us
    ppermute x3, starting transfers between devices, core_swap(): return lax.ppermute(value, 'c', [(0, 1), (1, 0)])  5.87 us
    ppermute x3, waiting for transfers between devices, core_swap(): return lax.ppermute(value, 'c', [(0, 1), (1, 0)])  4.8 us
  transfers between devices with their start and end apart: 6, of which 5 were waited for; matrix products, arithmetic and copies ran while one was open for 2% of the time, Pallas kernels for 7%

profile of v3, /device:TPU:24, one launch (start us, length us, event | category | flops | bytes accessed | tf_op | source)
XLA Modules:
  0.0 167.7 jit_solution(8292810758474219904)
XLA Ops:
  7.2 0.0 copy-start
  7.2 0.0 all-gather.2.cloned.1.call-start
  7.2 1.3 dispatch.1
  8.6 28.4 %all_to_all.15 = bf16[32,24,256]{2,1,0:T(8,128)(2,1)} all-to-all(bf16[32,24,256]{2,1,0:T(8,128)(2,1)S(1)} %dispatch.1), channel_id=1, replica_groups=mesh['z'=8,'x'=4,'y'=8,'c'=2] {'z','x'}, dimensions={0} | all-to-all | bytes 786432 | tf_op jit(solution)/shard_map/all_to_all | solution.py:416
  36.9 0.0 all-gather.2.cloned.1.call-update
  37.0 0.0 copy-done
  37.0 1.2 fusion
  38.1 1.0 copy.15
  39.1 4.3 %all-to-all-start.1 = ((bf16[32,32,256]{2,1,0:T(8,128)(2,1)}), bf16[32,32,256]{2,1,0:T(8,128)(2,1)S(1)}, u32[]{:S(2)}, u32[]{:S(2)}) async-start(bf16[32,32,256]{2,1,0:T(8,128)(2,1)} %bitcast.8), calls=%async_computation.1 | async-start | bytes 1048576 | tf_op jit(solution)/shard_map/all_to_all | solution.py:424
  43.4 0.0 reduce-scatter.2.cloned.1.call-start
  43.5 2.3 %other_half.1 = bf16[3,64,2048]{2,1,0:T(8,128)(2,1)} custom-call(s32[1]{0:T(128)} %bitcast.c_ref, bf16[64,4096]{1,0:T(8,128)(2,1)} %bitcast.17, bf16[64,4096]{1,0:T(8,128)(2,1)} %bitcast.20, bf16[64,4096]{1,0:T(8,128)(2,1)} %bitcast.23), custom_call_target="tpu_custom_call" | custom-call | tf_op jit(solution)/shard_map/other_half/pallas_call | solution.py:78
  45.8 1.9 %collective-permute-start = (bf16[3,64,2048]{2,1,0:T(8,128)(2,1)}, bf16[3,64,2048]{2,1,0:T(8,128)(2,1)S(1)}, u32[]{:S(2)}, u32[]{:S(2)}) collective-permute-start(bf16[3,64,2048]{2,1,0:T(8,128)(2,1)} %other_half.1), channel_id=1, source_target_pairs={{0,1},{1,0},{2,3},{3,2},{4,5},{5,4},{6,7},{7,6},{8,9},{9,8},{10,11... | collective-permute-start | bytes 2359304 | tf_op jit(solution)/shard_map/ppermute | solution.py:408
  47.7 12.8 %all-to-all-done.1 = bf16[32,32,256]{2,1,0:T(8,128)(2,1)S(1)} async-done(((bf16[32,32,256]{2,1,0:T(8,128)(2,1)}), bf16[32,32,256]{2,1,0:T(8,128)(2,1)S(1)}, u32[]{:S(2)}, u32[]{:S(2)}) %all-to-all-start.1) | async-done | bytes 524320 | tf_op jit(solution)/shard_map/all_to_all | solution.py:424
  60.6 0.7 convert_reduce_fusion
  61.3 0.0 collective-permute-done.wr_far
  61.3 0.0 copy-start.1
  61.3 18.4 %all-gather.2.cloned.1.call-done.xg_far = bf16[8,768,256]{2,1,0:T(8,128)(2,1)} async-done(((bf16[1,768,256]{2,1,0:T(8,128)(2,1)}), bf16[8,768,256]{2,1,0:T(8,128)(2,1)}) %all-gather.2.cloned.1.call-update) | async-done | bytes 3145744 | tf_op jit(solution)/shard_map/all_gather | solution.py:418
  79.7 0.0 copy-done.1
  79.7 5.4 %forward.1.own_far = f32[256,768]{1,0:T(8,128)} custom-call(s32[1]{0:T(128)} %bitcast.c_ref, bf16[8,768,256]{2,1,0:T(8,128)(2,1)} %all-gather.2.cloned.1.call-done.xg_far, bf16[64,4096]{1,0:T(8,128)(2,1)} %bitcast.18, bf16[64,4096]{1,0:T(8,128)(2,1)} %bitcast.21, bf16[64,4096]{1,0:T(8,128)(2,1)} %bitcast.24, bf16[3,64,2048]{2,1,0:T(8,128)(2,1)} %copy-done.1), custom_call_target="tpu_custom_call" | custom-call | tf_op jit(solution)/shard_map/forward/pallas_call | solution.py:78
  85.1 1.9 %collective-permute-start.1 = (f32[256,768]{1,0:T(8,128)}, f32[256,768]{1,0:T(8,128)S(1)}, u32[]{:S(2)}, u32[]{:S(2)}) collective-permute-start(f32[256,768]{1,0:T(8,128)} %forward.1.own_far), channel_id=1, source_target_pairs={{0,1},{1,0},{2,3},{3,2},{4,5},{5,4},{6,7},{7,6},{8,9},{9,8},{10,11... | collective-permute-start | bytes 2359304 | tf_op jit(solution)/shard_map/ppermute | solution.py:408
  87.1 2.5 %collective-permute-done.1.got_ref = f32[256,768]{1,0:T(8,128)S(1)} collective-permute-done((f32[256,768]{1,0:T(8,128)}, f32[256,768]{1,0:T(8,128)S(1)}, u32[]{:S(2)}, u32[]{:S(2)}) %collective-permute-start.1) | collective-permute-done | bytes 786464 | tf_op jit(solution)/shard_map/ppermute | solution.py:408
  89.5 4.3 %backward.1 = (bf16[8,392,256]{2,1,0:T(8,128)(2,1)}, bf16[2,192,768]{2,1,0:T(8,128)(2,1)}) custom-call(s32[1]{0:T(128)} %bitcast.c_ref, f32[256,768]{1,0:T(8,128)} %forward.1.own_far, bf16[64,4096]{1,0:T(8,128)(2,1)} %bitcast.19, bf16[64,4096]{1,0:T(8,128)(2,1)} %bitcast.22, bf16[3,64,2048]{2,1,0:T(8,128)(2,1)} %copy-done.1, ...), custom_call_target="tpu_custom_call" | custom-call | tf_op jit(solution)/shard_map/backward/pallas_call | solution.py:78
  93.9 0.0 reduce-scatter.2.cloned.1.call-update
  93.9 4.5 %partner_grads.1 = bf16[192,2048]{1,0:T(8,128)(2,1)} custom-call(bf16[2,192,768]{2,1,0:T(8,128)(2,1)} %get-tuple-element.33.left_far, bf16[8,768,256]{2,1,0:T(8,128)(2,1)} %all-gather.2.cloned.1.call-done.xg_far), custom_call_target="tpu_custom_call" | custom-call | tf_op jit(solution)/shard_map/partner_grads/pallas_call | solution.py:78
  98.3 2.0 %collective-permute-start.2 = (bf16[192,2048]{1,0:T(8,128)(2,1)}, bf16[192,2048]{1,0:T(8,128)(2,1)S(1)}, u32[]{:S(2)}, u32[]{:S(2)}) collective-permute-start(bf16[192,2048]{1,0:T(8,128)(2,1)} %partner_grads.1), channel_id=1, source_target_pairs={{0,1},{1,0},{2,3},{3,2},{4,5},{5,4},{6,7},{7,6},{8,9},{9,8},{10,11... | collective-permute-start | bytes 2359304 | tf_op jit(solution)/shard_map/ppermute | solution.py:408
  100.4 2.3 %collective-permute-done.2.got_far = bf16[192,2048]{1,0:T(8,128)(2,1)S(1)} collective-permute-done((bf16[192,2048]{1,0:T(8,128)(2,1)}, bf16[192,2048]{1,0:T(8,128)(2,1)S(1)}, u32[]{:S(2)}, u32[]{:S(2)}) %collective-permute-start.2) | collective-permute-done | bytes 786464 | tf_op jit(solution)/shard_map/ppermute | solution.py:408
  102.7 0.0 copy-start.2
  102.7 0.9 copy-done.2
  103.6 4.8 %merged_grads.1 = (f32[64,4096]{1,0:T(8,128)}, f32[64,4096]{1,0:T(8,128)}, f32[64,4096]{1,0:T(8,128)}) custom-call(s32[1]{0:T(128)} %bitcast.c_ref, bf16[2,192,768]{2,1,0:T(8,128)(2,1)} %get-tuple-element.33.left_far, bf16[8,768,256]{2,1,0:T(8,128)(2,1)} %all-gather.2.cloned.1.call-done.xg_far, bf16[192,2048]{1,0:T(8,128)(2,1)} %copy-done.2), custom_call_target="tpu_custom_call" | custom-call | tf_op jit(solution)/shard_map/merged_grads/pallas_call | solution.py:78
  108.4 27.9 %reduce-scatter.2.cloned.1.call-done = bf16[1,392,256]{2,1,0:T(8,128)(2,1)} async-done(((bf16[8,392,256]{2,1,0:T(8,128)(2,1)}), bf16[1,392,256]{2,1,0:T(8,128)(2,1)}) %reduce-scatter.2.cloned.1.call-update) | async-done | bytes 200720 | tf_op jit(solution)/shard_map/reduce_scatter | solution.py:432
  136.3 1.4 placed_rows.1
  137.7 21.4 %all_to_all.16.back_ref = bf16[32,16,256]{2,1,0:T(8,128)(2,1)S(1)} all-to-all(bf16[32,16,256]{2,1,0:T(8,128)(2,1)S(1)} %placed_rows.1), channel_id=1, replica_groups=mesh['z'=8,'x'=4,'y'=8,'c'=2] {'z','x'}, dimensions={0} | all-to-all | bytes 524288 | tf_op jit(solution)/shard_map/all_to_all | solution.py:436
  159.1 1.7 %combine.1 = (bf16[128,256]{1,0:T(8,128)(2,1)}, f32[2,128]{1,0:T(2,128)}) custom-call(bf16[32,16,256]{2,1,0:T(8,128)(2,1)S(1)} %all_to_all.16.back_ref, s32[2,128]{1,0:T(2,128)} %bitcast.28, f32[2,128]{1,0:T(2,128)} %bitcast.30), custom_call_target="tpu_custom_call" | custom-call | tf_op jit(solution)/shard_map/combine/pallas_call | solution.py:78
Async XLA Ops:
  7.2 29.8 %copy-start = (bf16[128,1024]{1,0:T(8,128)(2,1)S(1)}, bf16[128,1024]{1,0:T(8,128)(2,1)}, u32[]{:S(2)}) copy-start(bf16[128,1024]{1,0:T(8,128)(2,1)} %param.15) | copy-start | bytes 786436
  7.2 72.5 %all-gather.2.cloned.1.call-start = ((), (), s32[]{:S(2)}) async-start(), calls=%async_computation.4 | async-start | bytes 3538944 | tf_op jit(solution)/shard_map/all_gather | solution.py:418
  39.1 21.4 %all-to-all-start.1 = ((bf16[32,32,256]{2,1,0:T(8,128)(2,1)}), bf16[32,32,256]{2,1,0:T(8,128)(2,1)S(1)}, u32[]{:S(2)}, u32[]{:S(2)}) async-start(bf16[32,32,256]{2,1,0:T(8,128)(2,1)} %bitcast.8), calls=%async_computation.1 | async-start | bytes 1048576 | tf_op jit(solution)/shard_map/all_to_all | solution.py:424
  43.4 92.9 %reduce-scatter.2.cloned.1.call-start = ((), (), s32[]{:S(2)}) async-start(), calls=%async_computation.5 | async-start | bytes 1806336 | tf_op jit(solution)/shard_map/reduce_scatter | solution.py:432
  45.8 15.4 %collective-permute-start = (bf16[3,64,2048]{2,1,0:T(8,128)(2,1)}, bf16[3,64,2048]{2,1,0:T(8,128)(2,1)S(1)}, u32[]{:S(2)}, u32[]{:S(2)}) collective-permute-start(bf16[3,64,2048]{2,1,0:T(8,128)(2,1)} %other_half.1), channel_id=1, source_target_pairs={{0,1},{1,0},{2,3},{3,2},{4,5},{5,4},{6,7},{7,6},{8,9},{9,8},{10,11... | collective-permute-start | bytes 2359304 | tf_op jit(solution)/shard_map/ppermute | solution.py:408
  61.3 18.4 %copy-start.1 = (bf16[3,64,2048]{2,1,0:T(8,128)(2,1)}, bf16[3,64,2048]{2,1,0:T(8,128)(2,1)S(1)}, u32[]{:S(2)}) copy-start(bf16[3,64,2048]{2,1,0:T(8,128)(2,1)S(1)} %collective-permute-done.wr_far) | copy-start | bytes 2359300
  85.1 4.4 %collective-permute-start.1 = (f32[256,768]{1,0:T(8,128)}, f32[256,768]{1,0:T(8,128)S(1)}, u32[]{:S(2)}, u32[]{:S(2)}) collective-permute-start(f32[256,768]{1,0:T(8,128)} %forward.1.own_far), channel_id=1, source_target_pairs={{0,1},{1,0},{2,3},{3,2},{4,5},{5,4},{6,7},{7,6},{8,9},{9,8},{10,11... | collective-permute-start | bytes 2359304 | tf_op jit(solution)/shard_map/ppermute | solution.py:408
  98.3 4.4 %collective-permute-start.2 = (bf16[192,2048]{1,0:T(8,128)(2,1)}, bf16[192,2048]{1,0:T(8,128)(2,1)S(1)}, u32[]{:S(2)}, u32[]{:S(2)}) collective-permute-start(bf16[192,2048]{1,0:T(8,128)(2,1)} %partner_grads.1), channel_id=1, source_target_pairs={{0,1},{1,0},{2,3},{3,2},{4,5},{5,4},{6,7},{7,6},{8,9},{9,8},{10,11... | collective-permute-start | bytes 2359304 | tf_op jit(solution)/shard_map/ppermute | solution.py:408
  102.7 0.9 copy-start.2
Sparse Core Ops, SparseCore 0:
  37.1 42.5 all-gather.1
  94.0 42.2 reduce-scatter.1

commit v4 on v3

--- a/solution.py
+++ b/solution.py
@@ -123,21 +123,23 @@
 
 
 def forward_kernel(
-    c_ref, xg_far, wg_far, wu_far, wd_far, wr_far, out_ref, xg_ref, wg_ref, wu_ref, wd_ref, wr_ref, sems
+    c_ref, xg_far, wg_far, wu_far, wd_far, wr_far, out_ref, xg_ref, own_ref, wr_ref, sems
 ):
-    weights = [(wg_far, wg_ref), (wd_far, wd_ref), (wu_far, wu_ref), (wr_far, wr_ref)]
-    blocks = [(xg_far.at[y], xg_ref.at[y]) for y in range(NY)]
-    copies = fetch(blocks[:1] + weights + blocks[1:], sems)
-    for copy in copies[:5]:
-        copy.wait()
+    pairs = []
+    for y in range(NY):
+        pairs.append((xg_far.at[y], xg_ref.at[y]))
+        pairs.append((wr_far.at[:, :, half_lanes(y)], wr_ref.at[:, :, half_lanes(y)]))
+        for at, far in enumerate((wg_far, wu_far, wd_far)):
+            pairs.append((far.at[:, lanes_of(y, c_ref[0])], own_ref.at[at, :, half_lanes(y)]))
+    copies = fetch(pairs, sems)
     total = None
     for y in range(NY):
-        if y > 0:
-            copies[4 + y].wait()
+        for copy in copies[5 * y : 5 * y + 5]:
+            copy.wait()
         parts = []
-        for at, ref in enumerate((wg_ref, wd_ref, wu_ref)):
-            parts.append(ref[:, lanes_of(y, c_ref[0])])
-            parts.append(wr_ref[(0, 2, 1)[at], :, half_lanes(y)])
+        for at in (0, 2, 1):
+            parts.append(own_ref[at, :, half_lanes(y)])
+            parts.append(wr_ref[at, :, half_lanes(y)])
         part = lax.dot_general(
             jnp.concatenate(parts, axis=0),
             xg_ref[y],
@@ -148,12 +150,12 @@
     pair = 2 * HID
     out_ref[0:pair, :] = jnp.where(
         is_token_lane((pair, ROWS)), total[0:pair, :], total[pair : 2 * pair, :]
-    )
-    out_ref[pair : 2 * pair, :] = total[2 * pair : 3 * pair, :]
+    ).astype(BF16)
+    out_ref[pair : 2 * pair, :] = total[2 * pair : 3 * pair, :].astype(BF16)
 
 
 def forward(core, xg, wg, wu, wd, wr):
-    out = (jax.ShapeDtypeStruct((4 * HID, ROWS), F32),)
+    out = (pltpu.VMEM((4 * HID, ROWS), BF16),)
     return kernel_call(
         forward_kernel,
         out,
@@ -162,36 +164,32 @@
         far=(xg, wg, wu, wd, wr),
         scratch=(
             pltpu.VMEM((NY, ROWS, WIDTH), BF16),
-            pltpu.VMEM((HID, 2 * HALF), BF16),
-            pltpu.VMEM((HID, 2 * HALF), BF16),
-            pltpu.VMEM((HID, 2 * HALF), BF16),
             pltpu.VMEM((3, HID, HALF), BF16),
-            flags(4 + NY),
+            pltpu.VMEM((3, HID, HALF), BF16),
+            flags(5 * NY),
         ),
     )[0]
 
 
 def backward_kernel(
-    c_ref, own_far, wg_far, wu_far, wr_far, got_ref, out_far, left_ref,
-    own_ref, wg_ref, wu_ref, wr_ref, out_ref, sems, out_sems,
+    c_ref, wg_far, wu_far, wr_far, own_ref, got_ref, out_far, left_ref,
+    wg_ref, wu_ref, wr_ref, out_ref, sems, out_sems,
 ):
     copies = fetch(
         [
-            (own_far, own_ref),
             (wg_far, wg_ref),
             (wu_far, wu_ref),
             (wr_far.at[0:2], wr_ref),
         ],
         sems,
     )
-    copies[0].wait()
 
     def total(at):
         low, mid, high = 2 * at * HID, (2 * at + 1) * HID, (2 * at + 2) * HID
         return jnp.concatenate(
             [
-                own_ref[low:mid, :] + got_ref[mid:high, :],
-                own_ref[mid:high, :] + got_ref[low:mid, :],
+                own_ref[low:mid, :].astype(F32) + got_ref[mid:high, :].astype(F32),
+                own_ref[mid:high, :].astype(F32) + got_ref[low:mid, :].astype(F32),
             ],
             axis=0,
         )
@@ -220,7 +218,7 @@
     grads = lax.dot_general(
         compact, both, (((1,), (1,)), ((), ())), preferred_element_type=F32
     ).astype(BF16)
-    for copy in copies[1:]:
+    for copy in copies:
         copy.wait()
     sent = []
     for y in range(NY):
@@ -251,16 +249,15 @@
         out,
         "backward",
         core=core,
-        far=(own, wg, wu, wr),
-        near=(got,),
+        far=(wg, wu, wr),
+        near=(own, got),
         far_out=1,
         scratch=(
-            pltpu.VMEM((4 * HID, ROWS), F32),
             pltpu.VMEM((HID, 2 * HALF), BF16),
             pltpu.VMEM((HID, 2 * HALF), BF16),
             pltpu.VMEM((2, HID, HALF), BF16),
             pltpu.VMEM((NY, BACK, WIDTH), BF16),
-            flags(4),
+            flags(3),
             flags(NY),
         ),
     )

time: 168 us -> 166 us (0.988)
  no operation moved by 1% of the time
where the time goes in v4:
time: 166 us
  waiting for transfers between devices  63.2 us (38%)
  blocking collectives  49.8 us (30%)
  Pallas kernels  24.4 us (15%)
  between operations  14.1 us (8%)
  starting transfers between devices  10.3 us (6%)
  local copies, waits for them, and re-layouts  1.92 us (1%)
    all_to_all x1, blocking collectives, shards(): rows = lax.all_to_all(sent, EP, split_axis=0, concat_axis=0, tiled=True)  28.4 us
    reduce_scatter x1, waiting for transfers between devices, shards(): got = lax.psum_scatter(parts, 'y', scatter_dimension=0, tiled=False)  27.8 us
    pallas_call x8, Pallas kernels, kernel_call(): pl.pallas_call(body, in_specs=specs, out_specs=results, out_shape=list(ou...  24.4 us
    all_to_all x1, blocking collectives, shards(): lax.all_to_all(placed_rows(got), EP, split_axis=0, concat_axis=0, tiled=T...  21.4 us
    all_gather x1, waiting for transfers between devices, shards(): xg = lax.all_gather(rows.reshape(ROWS, WIDTH), 'y', axis=0, tiled=False)  18.4 us
    all_to_all x1, waiting for transfers between devices, shards(): lax.all_to_all(shared.reshape(EXPERTS, -1, WIDTH), EP, split_axis=0, conc...  12.8 us
    ppermute x3, starting transfers between devices, core_swap(): return lax.ppermute(value, 'c', [(0, 1), (1, 0)])  5.88 us
    all_to_all x1, starting transfers between devices, shards(): lax.all_to_all(shared.reshape(EXPERTS, -1, WIDTH), EP, split_axis=0, conc...  4.3 us
  transfers between devices with their start and end apart: 6, of which 5 were waited for; matrix products, arithmetic and copies ran while one was open for 2% of the time, Pallas kernels for 7%

profile of v4, /device:TPU:24, one launch (start us, length us, event | category | flops | bytes accessed | tf_op | source)
XLA Modules:
  0.0 165.5 jit_solution(17931363640116606916)
XLA Ops:
  7.2 0.0 copy-start
  7.2 0.0 all-gather.2.cloned.1.call-start
  7.2 1.3 dispatch.1
  8.6 28.4 %all_to_all.15 = bf16[32,24,256]{2,1,0:T(8,128)(2,1)} all-to-all(bf16[32,24,256]{2,1,0:T(8,128)(2,1)S(1)} %dispatch.1), channel_id=1, replica_groups=mesh['z'=8,'x'=4,'y'=8,'c'=2] {'z','x'}, dimensions={0} | all-to-all | bytes 786432 | tf_op jit(solution)/shard_map/all_to_all | solution.py:413
  36.9 0.0 all-gather.2.cloned.1.call-update
  37.0 0.0 copy-done
  37.0 1.2 fusion
  38.1 1.0 copy.15
  39.1 4.3 %all-to-all-start.1 = ((bf16[32,32,256]{2,1,0:T(8,128)(2,1)}), bf16[32,32,256]{2,1,0:T(8,128)(2,1)S(1)}, u32[]{:S(2)}, u32[]{:S(2)}) async-start(bf16[32,32,256]{2,1,0:T(8,128)(2,1)} %bitcast.8), calls=%async_computation.1 | async-start | bytes 1048576 | tf_op jit(solution)/shard_map/all_to_all | solution.py:421
  43.4 0.0 reduce-scatter.2.cloned.1.call-start
  43.5 2.3 %other_half.1 = bf16[3,64,2048]{2,1,0:T(8,128)(2,1)} custom-call(s32[1]{0:T(128)} %bitcast.c_ref, bf16[64,4096]{1,0:T(8,128)(2,1)} %bitcast.17, bf16[64,4096]{1,0:T(8,128)(2,1)} %bitcast.20, bf16[64,4096]{1,0:T(8,128)(2,1)} %bitcast.23), custom_call_target="tpu_custom_call" | custom-call | tf_op jit(solution)/shard_map/other_half/pallas_call | solution.py:78
  45.8 1.9 %collective-permute-start = (bf16[3,64,2048]{2,1,0:T(8,128)(2,1)}, bf16[3,64,2048]{2,1,0:T(8,128)(2,1)S(1)}, u32[]{:S(2)}, u32[]{:S(2)}) collective-permute-start(bf16[3,64,2048]{2,1,0:T(8,128)(2,1)} %other_half.1), channel_id=1, source_target_pairs={{0,1},{1,0},{2,3},{3,2},{4,5},{5,4},{6,7},{7,6},{8,9},{9,8},{10,11... | collective-permute-start | bytes 2359304 | tf_op jit(solution)/shard_map/ppermute | solution.py:405
  47.7 12.8 %all-to-all-done.1 = bf16[32,32,256]{2,1,0:T(8,128)(2,1)S(1)} async-done(((bf16[32,32,256]{2,1,0:T(8,128)(2,1)}), bf16[32,32,256]{2,1,0:T(8,128)(2,1)S(1)}, u32[]{:S(2)}, u32[]{:S(2)}) %all-to-all-start.1) | async-done | bytes 524320 | tf_op jit(solution)/shard_map/all_to_all | solution.py:421
  60.6 0.7 convert_reduce_fusion
  61.3 0.0 collective-permute-done.wr_far
  61.3 0.0 copy-start.1
  61.3 18.4 %all-gather.2.cloned.1.call-done.xg_far = bf16[8,768,256]{2,1,0:T(8,128)(2,1)} async-done(((bf16[1,768,256]{2,1,0:T(8,128)(2,1)}), bf16[8,768,256]{2,1,0:T(8,128)(2,1)}) %all-gather.2.cloned.1.call-update) | async-done | bytes 3145744 | tf_op jit(solution)/shard_map/all_gather | solution.py:415
  79.7 0.0 copy-done.1
  79.7 4.2 %forward.1.own_ref = bf16[256,768]{1,0:T(8,128)(2,1)S(1)} custom-call(s32[1]{0:T(128)} %bitcast.c_ref, bf16[8,768,256]{2,1,0:T(8,128)(2,1)} %all-gather.2.cloned.1.call-done.xg_far, bf16[64,4096]{1,0:T(8,128)(2,1)} %bitcast.18, bf16[64,4096]{1,0:T(8,128)(2,1)} %bitcast.21, bf16[64,4096]{1,0:T(8,128)(2,1)} %bitcast.24, bf16[3,64,2048]{2,1,0:T(8,128)(2,1)} %copy-done.1), custom_call_target="tpu_custom_call" | custom-call | tf_op jit(solution)/shard_map/forward/pallas_call | solution.py:78
  83.9 1.9 %collective-permute-start.1 = (bf16[256,768]{1,0:T(8,128)(2,1)S(1)}, bf16[256,768]{1,0:T(8,128)(2,1)S(1)}, u32[]{:S(2)}, u32[]{:S(2)}) collective-permute-start(bf16[256,768]{1,0:T(8,128)(2,1)S(1)} %forward.1.own_ref), channel_id=1, source_target_pairs={{0,1},{1,0},{2,3},{3,2},{4,5},{5,4},{6,7},{7,6},{8,9},{9,8},{10,11... | collective-permute-start | bytes 1179656 | tf_op jit(solution)/shard_map/ppermute | solution.py:405
  85.9 1.7 %collective-permute-done.1.got_ref = bf16[256,768]{1,0:T(8,128)(2,1)S(1)} collective-permute-done((bf16[256,768]{1,0:T(8,128)(2,1)S(1)}, bf16[256,768]{1,0:T(8,128)(2,1)S(1)}, u32[]{:S(2)}, u32[]{:S(2)}) %collective-permute-start.1) | collective-permute-done | bytes 393248 | tf_op jit(solution)/shard_map/ppermute | solution.py:405
  87.5 4.2 %backward.1 = (bf16[8,392,256]{2,1,0:T(8,128)(2,1)}, bf16[2,192,768]{2,1,0:T(8,128)(2,1)}) custom-call(s32[1]{0:T(128)} %bitcast.c_ref, bf16[64,4096]{1,0:T(8,128)(2,1)} %bitcast.19, bf16[64,4096]{1,0:T(8,128)(2,1)} %bitcast.22, bf16[3,64,2048]{2,1,0:T(8,128)(2,1)} %copy-done.1, bf16[256,768]{1,0:T(8,128)(2,1)S(1)} %forward.1.own_ref, ...), custom_call_target="tpu_custom_call" | custom-call | tf_op jit(solution)/shard_map/backward/pallas_call | solution.py:78
  91.7 0.0 reduce-scatter.2.cloned.1.call-update
  91.7 4.5 %partner_grads.1 = bf16[192,2048]{1,0:T(8,128)(2,1)} custom-call(bf16[2,192,768]{2,1,0:T(8,128)(2,1)} %get-tuple-element.33.left_far, bf16[8,768,256]{2,1,0:T(8,128)(2,1)} %all-gather.2.cloned.1.call-done.xg_far), custom_call_target="tpu_custom_call" | custom-call | tf_op jit(solution)/shard_map/partner_grads/pallas_call | solution.py:78
  96.2 2.0 %collective-permute-start.2 = (bf16[192,2048]{1,0:T(8,128)(2,1)}, bf16[192,2048]{1,0:T(8,128)(2,1)S(1)}, u32[]{:S(2)}, u32[]{:S(2)}) collective-permute-start(bf16[192,2048]{1,0:T(8,128)(2,1)} %partner_grads.1), channel_id=1, source_target_pairs={{0,1},{1,0},{2,3},{3,2},{4,5},{5,4},{6,7},{7,6},{8,9},{9,8},{10,11... | collective-permute-start | bytes 2359304 | tf_op jit(solution)/shard_map/ppermute | solution.py:405
  98.3 2.3 %collective-permute-done.2.got_far = bf16[192,2048]{1,0:T(8,128)(2,1)S(1)} collective-permute-done((bf16[192,2048]{1,0:T(8,128)(2,1)}, bf16[192,2048]{1,0:T(8,128)(2,1)S(1)}, u32[]{:S(2)}, u32[]{:S(2)}) %collective-permute-start.2) | collective-permute-done | bytes 786464 | tf_op jit(solution)/shard_map/ppermute | solution.py:405
  100.6 0.0 copy-start.2
  100.6 0.9 copy-done.2
  101.5 4.8 %merged_grads.1 = (f32[64,4096]{1,0:T(8,128)}, f32[64,4096]{1,0:T(8,128)}, f32[64,4096]{1,0:T(8,128)}) custom-call(s32[1]{0:T(128)} %bitcast.c_ref, bf16[2,192,768]{2,1,0:T(8,128)(2,1)} %get-tuple-element.33.left_far, bf16[8,768,256]{2,1,0:T(8,128)(2,1)} %all-gather.2.cloned.1.call-done.xg_far, bf16[192,2048]{1,0:T(8,128)(2,1)} %copy-done.2), custom_call_target="tpu_custom_call" | custom-call | tf_op jit(solution)/shard_map/merged_grads/pallas_call | solution.py:78
  106.3 27.8 %reduce-scatter.2.cloned.1.call-done = bf16[1,392,256]{2,1,0:T(8,128)(2,1)} async-done(((bf16[8,392,256]{2,1,0:T(8,128)(2,1)}), bf16[1,392,256]{2,1,0:T(8,128)(2,1)}) %reduce-scatter.2.cloned.1.call-update) | async-done | bytes 200720 | tf_op jit(solution)/shard_map/reduce_scatter | solution.py:429
  134.1 1.4 placed_rows.1
  135.5 21.4 %all_to_all.16.back_ref = bf16[32,16,256]{2,1,0:T(8,128)(2,1)S(1)} all-to-all(bf16[32,16,256]{2,1,0:T(8,128)(2,1)S(1)} %placed_rows.1), channel_id=1, replica_groups=mesh['z'=8,'x'=4,'y'=8,'c'=2] {'z','x'}, dimensions={0} | all-to-all | bytes 524288 | tf_op jit(solution)/shard_map/all_to_all | solution.py:433
  157.0 1.7 %combine.1 = (bf16[128,256]{1,0:T(8,128)(2,1)}, f32[2,128]{1,0:T(2,128)}) custom-call(bf16[32,16,256]{2,1,0:T(8,128)(2,1)S(1)} %all_to_all.16.back_ref, s32[2,128]{1,0:T(2,128)} %bitcast.28, f32[2,128]{1,0:T(2,128)} %bitcast.30), custom_call_target="tpu_custom_call" | custom-call | tf_op jit(solution)/shard_map/combine/pallas_call | solution.py:78
Async XLA Ops:
  7.2 29.8 %copy-start = (bf16[128,1024]{1,0:T(8,128)(2,1)S(1)}, bf16[128,1024]{1,0:T(8,128)(2,1)}, u32[]{:S(2)}) copy-start(bf16[128,1024]{1,0:T(8,128)(2,1)} %param.15) | copy-start | bytes 786436
  7.2 72.5 %all-gather.2.cloned.1.call-start = ((), (), s32[]{:S(2)}) async-start(), calls=%async_computation.4 | async-start | bytes 3538944 | tf_op jit(solution)/shard_map/all_gather | solution.py:415
  39.1 21.4 %all-to-all-start.1 = ((bf16[32,32,256]{2,1,0:T(8,128)(2,1)}), bf16[32,32,256]{2,1,0:T(8,128)(2,1)S(1)}, u32[]{:S(2)}, u32[]{:S(2)}) async-start(bf16[32,32,256]{2,1,0:T(8,128)(2,1)} %bitcast.8), calls=%async_computation.1 | async-start | bytes 1048576 | tf_op jit(solution)/shard_map/all_to_all | solution.py:421
  43.4 90.7 %reduce-scatter.2.cloned.1.call-start = ((), (), s32[]{:S(2)}) async-start(), calls=%async_computation.5 | async-start | bytes 1806336 | tf_op jit(solution)/shard_map/reduce_scatter | solution.py:429
  45.8 15.4 %collective-permute-start = (bf16[3,64,2048]{2,1,0:T(8,128)(2,1)}, bf16[3,64,2048]{2,1,0:T(8,128)(2,1)S(1)}, u32[]{:S(2)}, u32[]{:S(2)}) collective-permute-start(bf16[3,64,2048]{2,1,0:T(8,128)(2,1)} %other_half.1), channel_id=1, source_target_pairs={{0,1},{1,0},{2,3},{3,2},{4,5},{5,4},{6,7},{7,6},{8,9},{9,8},{10,11... | collective-permute-start | bytes 2359304 | tf_op jit(solution)/shard_map/ppermute | solution.py:405
  61.3 18.4 %copy-start.1 = (bf16[3,64,2048]{2,1,0:T(8,128)(2,1)}, bf16[3,64,2048]{2,1,0:T(8,128)(2,1)S(1)}, u32[]{:S(2)}) copy-start(bf16[3,64,2048]{2,1,0:T(8,128)(2,1)S(1)} %collective-permute-done.wr_far) | copy-start | bytes 2359300
  83.9 3.6 %collective-permute-start.1 = (bf16[256,768]{1,0:T(8,128)(2,1)S(1)}, bf16[256,768]{1,0:T(8,128)(2,1)S(1)}, u32[]{:S(2)}, u32[]{:S(2)}) collective-permute-start(bf16[256,768]{1,0:T(8,128)(2,1)S(1)} %forward.1.own_ref), channel_id=1, source_target_pairs={{0,1},{1,0},{2,3},{3,2},{4,5},{5,4},{6,7},{7,6},{8,9},{9,8},{10,11... | collective-permute-start | bytes 1179656 | tf_op jit(solution)/shard_map/ppermute | solution.py:405
  96.2 4.4 %collective-permute-start.2 = (bf16[192,2048]{1,0:T(8,128)(2,1)}, bf16[192,2048]{1,0:T(8,128)(2,1)S(1)}, u32[]{:S(2)}, u32[]{:S(2)}) collective-permute-start(bf16[192,2048]{1,0:T(8,128)(2,1)} %partner_grads.1), channel_id=1, source_target_pairs={{0,1},{1,0},{2,3},{3,2},{4,5},{5,4},{6,7},{7,6},{8,9},{9,8},{10,11... | collective-permute-start | bytes 2359304 | tf_op jit(solution)/shard_map/ppermute | solution.py:405
  100.6 0.9 copy-start.2
Sparse Core Ops, SparseCore 0:
  37.1 42.5 all-gather.1
  91.9 42.2 reduce-scatter.1

commit v5 on v4

--- a/solution.py
+++ b/solution.py
@@ -172,8 +172,8 @@
 
 
 def backward_kernel(
-    c_ref, wg_far, wu_far, wr_far, own_ref, got_ref, out_far, left_ref,
-    wg_ref, wu_ref, wr_ref, out_ref, sems, out_sems,
+    c_ref, wg_far, wu_far, wr_far, own_ref, got_ref, out_far, left_far,
+    wg_ref, wu_ref, wr_ref, out_ref, left_ref, sems, out_sems,
 ):
     copies = fetch(
         [
@@ -211,6 +211,8 @@
         grad = grad.astype(BF16)
         left_ref[0, at * HID : (at + 1) * HID, :] = grad[0:HID]
         left_ref[1, at * HID : (at + 1) * HID, :] = grad[HID : 2 * HID]
+    sent = [pltpu.make_async_copy(left_ref, left_far, out_sems.at[NY])]
+    sent[0].start()
     both = jnp.concatenate([grad_gate.astype(BF16), grad_up.astype(BF16)], axis=0)
     slot = iota((SLOTS, ROWS), 0)
     lane = iota((SLOTS, ROWS), 1)
@@ -220,7 +222,6 @@
     ).astype(BF16)
     for copy in copies:
         copy.wait()
-    sent = []
     for y in range(NY):
         mats = jnp.concatenate(
             [
@@ -234,7 +235,7 @@
         out_ref[y, 0:SLOTS, :] = jnp.dot(grads, mats, preferred_element_type=F32).astype(BF16)
         out_ref[y, SLOTS:BACK, :] = tail
         sent.append(pltpu.make_async_copy(out_ref.at[y], out_far.at[y], out_sems.at[y]))
-        sent[y].start()
+        sent[-1].start()
     for copy in sent:
         copy.wait()
 
@@ -251,14 +252,15 @@
         core=core,
         far=(wg, wu, wr),
         near=(own, got),
-        far_out=1,
+        far_out=2,
         scratch=(
             pltpu.VMEM((HID, 2 * HALF), BF16),
             pltpu.VMEM((HID, 2 * HALF), BF16),
             pltpu.VMEM((2, HID, HALF), BF16),
             pltpu.VMEM((NY, BACK, WIDTH), BF16),
+            pltpu.VMEM((2, 3 * HID, ROWS), BF16),
             flags(3),
-            flags(NY),
+            flags(NY + 1),
         ),
     )
 
@@ -398,7 +400,7 @@
         jax.ShapeDtypeStruct((TOK, WIDTH), BF16),
         jax.ShapeDtypeStruct((TOP, TOK), F32),
     )
-    return kernel_call(combine_kernel, out, "combine", rt, gw, near=(back,))
+    return kernel_call(combine_kernel, out, "combine", near=(back, rt, gw))
 
 
 def core_swap(value):

time: 166 us -> 165 us (level)
  no operation moved by 1% of the time
where the time goes in v5:
time: 165 us; the launch traced here: 164 us
  waiting for transfers between devices  63.2 us (38%)
  blocking collectives  49.9 us (30%)
  Pallas kernels  23.1 us (14%)
  between operations  14.2 us (9%)
  starting transfers between devices  10.3 us (6%)
  local copies, waits for them, and re-layouts  1.93 us (1%)
    all_to_all x1, blocking collectives, shards(): rows = lax.all_to_all(sent, EP, split_axis=0, concat_axis=0, tiled=True)  28.4 us
    reduce_scatter x1, waiting for transfers between devices, shards(): got = lax.psum_scatter(parts, 'y', scatter_dimension=0, tiled=False)  27.9 us
    pallas_call x8, Pallas kernels, kernel_call(): pl.pallas_call(body, in_specs=specs, out_specs=results, out_shape=list(ou...  23.1 us
    all_to_all x1, blocking collectives, shards(): lax.all_to_all(placed_rows(got), EP, split_axis=0, concat_axis=0, tiled=T...  21.5 us
    all_gather x1, waiting for transfers between devices, shards(): xg = lax.all_gather(rows.reshape(ROWS, WIDTH), 'y', axis=0, tiled=False)  18.4 us
    all_to_all x1, waiting for transfers between devices, shards(): lax.all_to_all(shared.reshape(EXPERTS, -1, WIDTH), EP, split_axis=0, conc...  12.8 us
    ppermute x3, starting transfers between devices, core_swap(): return lax.ppermute(value, 'c', [(0, 1), (1, 0)])  5.87 us
    all_to_all x1, starting transfers between devices, shards(): lax.all_to_all(shared.reshape(EXPERTS, -1, WIDTH), EP, split_axis=0, conc...  4.3 us
  transfers between devices with their start and end apart: 6, of which 5 were waited for; matrix products, arithmetic and copies ran while one was open for 2% of the time, Pallas kernels for 7%

profile of v5, /device:TPU:24, one launch (start us, length us, event | category | flops | bytes accessed | tf_op | source)
XLA Modules:
  0.0 164.4 jit_solution(11641754120524007995)
XLA Ops:
  7.2 0.0 copy-start
  7.2 0.0 all-gather.2.cloned.1.call-start
  7.2 1.3 dispatch.1
  8.6 28.4 %all_to_all.15 = bf16[32,24,256]{2,1,0:T(8,128)(2,1)} all-to-all(bf16[32,24,256]{2,1,0:T(8,128)(2,1)S(1)} %dispatch.1), channel_id=1, replica_groups=mesh['z'=8,'x'=4,'y'=8,'c'=2] {'z','x'}, dimensions={0} | all-to-all | bytes 786432 | tf_op jit(solution)/shard_map/all_to_all | solution.py:415
  36.9 0.0 all-gather.2.cloned.1.call-update
  37.0 0.0 copy-done
  37.0 1.2 fusion
  38.1 1.0 copy.15
  39.1 4.3 %all-to-all-start.1 = ((bf16[32,32,256]{2,1,0:T(8,128)(2,1)}), bf16[32,32,256]{2,1,0:T(8,128)(2,1)S(1)}, u32[]{:S(2)}, u32[]{:S(2)}) async-start(bf16[32,32,256]{2,1,0:T(8,128)(2,1)} %bitcast.8), calls=%async_computation.1 | async-start | bytes 1048576 | tf_op jit(solution)/shard_map/all_to_all | solution.py:423
  43.4 0.0 reduce-scatter.2.cloned.1.call-start
  43.5 2.3 %other_half.1 = bf16[3,64,2048]{2,1,0:T(8,128)(2,1)} custom-call(s32[1]{0:T(128)} %bitcast.c_ref, bf16[64,4096]{1,0:T(8,128)(2,1)} %bitcast.21, bf16[64,4096]{1,0:T(8,128)(2,1)} %bitcast.24, bf16[64,4096]{1,0:T(8,128)(2,1)} %bitcast.27), custom_call_target="tpu_custom_call" | custom-call | tf_op jit(solution)/shard_map/other_half/pallas_call | solution.py:78
  45.8 1.9 %collective-permute-start = (bf16[3,64,2048]{2,1,0:T(8,128)(2,1)}, bf16[3,64,2048]{2,1,0:T(8,128)(2,1)S(1)}, u32[]{:S(2)}, u32[]{:S(2)}) collective-permute-start(bf16[3,64,2048]{2,1,0:T(8,128)(2,1)} %other_half.1), channel_id=1, source_target_pairs={{0,1},{1,0},{2,3},{3,2},{4,5},{5,4},{6,7},{7,6},{8,9},{9,8},{10,11... | collective-permute-start | bytes 2359304 | tf_op jit(solution)/shard_map/ppermute | solution.py:407
  47.7 12.8 %all-to-all-done.1 = bf16[32,32,256]{2,1,0:T(8,128)(2,1)S(1)} async-done(((bf16[32,32,256]{2,1,0:T(8,128)(2,1)}), bf16[32,32,256]{2,1,0:T(8,128)(2,1)S(1)}, u32[]{:S(2)}, u32[]{:S(2)}) %all-to-all-start.1) | async-done | bytes 524320 | tf_op jit(solution)/shard_map/all_to_all | solution.py:423
  60.6 0.7 convert_reduce_fusion
  61.3 0.0 collective-permute-done.wr_far
  61.3 0.0 copy-start.3
  61.3 18.4 %all-gather.2.cloned.1.call-done.xg_far = bf16[8,768,256]{2,1,0:T(8,128)(2,1)} async-done(((bf16[1,768,256]{2,1,0:T(8,128)(2,1)}), bf16[8,768,256]{2,1,0:T(8,128)(2,1)}) %all-gather.2.cloned.1.call-update) | async-done | bytes 3145744 | tf_op jit(solution)/shard_map/all_gather | solution.py:417
  79.7 0.0 copy-done.3
  79.7 4.2 %forward.1.own_ref = bf16[256,768]{1,0:T(8,128)(2,1)S(1)} custom-call(s32[1]{0:T(128)} %bitcast.c_ref, bf16[8,768,256]{2,1,0:T(8,128)(2,1)} %all-gather.2.cloned.1.call-done.xg_far, bf16[64,4096]{1,0:T(8,128)(2,1)} %bitcast.22, bf16[64,4096]{1,0:T(8,128)(2,1)} %bitcast.25, bf16[64,4096]{1,0:T(8,128)(2,1)} %bitcast.28, bf16[3,64,2048]{2,1,0:T(8,128)(2,1)} %copy-done.3), custom_call_target="tpu_custom_call" | custom-call | tf_op jit(solution)/shard_map/forward/pallas_call | solution.py:78
  83.9 1.9 %collective-permute-start.1 = (bf16[256,768]{1,0:T(8,128)(2,1)S(1)}, bf16[256,768]{1,0:T(8,128)(2,1)S(1)}, u32[]{:S(2)}, u32[]{:S(2)}) collective-permute-start(bf16[256,768]{1,0:T(8,128)(2,1)S(1)} %forward.1.own_ref), channel_id=1, source_target_pairs={{0,1},{1,0},{2,3},{3,2},{4,5},{5,4},{6,7},{7,6},{8,9},{9,8},{10,11... | collective-permute-start | bytes 1179656 | tf_op jit(solution)/shard_map/ppermute | solution.py:407
  85.9 1.7 %collective-permute-done.1.got_ref = bf16[256,768]{1,0:T(8,128)(2,1)S(1)} collective-permute-done((bf16[256,768]{1,0:T(8,128)(2,1)S(1)}, bf16[256,768]{1,0:T(8,128)(2,1)S(1)}, u32[]{:S(2)}, u32[]{:S(2)}) %collective-permute-start.1) | collective-permute-done | bytes 393248 | tf_op jit(solution)/shard_map/ppermute | solution.py:407
  87.5 3.6 %backward.1 = (bf16[8,392,256]{2,1,0:T(8,128)(2,1)}, bf16[2,192,768]{2,1,0:T(8,128)(2,1)}) custom-call(s32[1]{0:T(128)} %bitcast.c_ref, bf16[64,4096]{1,0:T(8,128)(2,1)} %bitcast.23, bf16[64,4096]{1,0:T(8,128)(2,1)} %bitcast.26, bf16[3,64,2048]{2,1,0:T(8,128)(2,1)} %copy-done.3, bf16[256,768]{1,0:T(8,128)(2,1)S(1)} %forward.1.own_ref, ...), custom_call_target="tpu_custom_call" | custom-call | tf_op jit(solution)/shard_map/backward/pallas_call | solution.py:78
  91.1 0.0 reduce-scatter.2.cloned.1.call-update
  91.1 4.5 %partner_grads.1 = bf16[192,2048]{1,0:T(8,128)(2,1)} custom-call(bf16[2,192,768]{2,1,0:T(8,128)(2,1)} %get-tuple-element.33.left_far, bf16[8,768,256]{2,1,0:T(8,128)(2,1)} %all-gather.2.cloned.1.call-done.xg_far), custom_call_target="tpu_custom_call" | custom-call | tf_op jit(solution)/shard_map/partner_grads/pallas_call | solution.py:78
  95.6 0.0 copy-start.1
  95.6 0.0 copy-start.2
  95.6 2.0 %collective-permute-start.2 = (bf16[192,2048]{1,0:T(8,128)(2,1)}, bf16[192,2048]{1,0:T(8,128)(2,1)S(1)}, u32[]{:S(2)}, u32[]{:S(2)}) collective-permute-start(bf16[192,2048]{1,0:T(8,128)(2,1)} %partner_grads.1), channel_id=1, source_target_pairs={{0,1},{1,0},{2,3},{3,2},{4,5},{5,4},{6,7},{7,6},{8,9},{9,8},{10,11... | collective-permute-start | bytes 2359304 | tf_op jit(solution)/shard_map/ppermute | solution.py:407
  97.7 2.3 %collective-permute-done.2.got_far = bf16[192,2048]{1,0:T(8,128)(2,1)S(1)} collective-permute-done((bf16[192,2048]{1,0:T(8,128)(2,1)}, bf16[192,2048]{1,0:T(8,128)(2,1)S(1)}, u32[]{:S(2)}, u32[]{:S(2)}) %collective-permute-start.2) | collective-permute-done | bytes 786464 | tf_op jit(solution)/shard_map/ppermute | solution.py:407
  100.0 0.0 copy-start.4
  100.0 0.9 copy-done.4
  100.9 4.8 %merged_grads.1 = (f32[64,4096]{1,0:T(8,128)}, f32[64,4096]{1,0:T(8,128)}, f32[64,4096]{1,0:T(8,128)}) custom-call(s32[1]{0:T(128)} %bitcast.c_ref, bf16[2,192,768]{2,1,0:T(8,128)(2,1)} %get-tuple-element.33.left_far, bf16[8,768,256]{2,1,0:T(8,128)(2,1)} %all-gather.2.cloned.1.call-done.xg_far, bf16[192,2048]{1,0:T(8,128)(2,1)} %copy-done.4), custom_call_target="tpu_custom_call" | custom-call | tf_op jit(solution)/shard_map/merged_grads/pallas_call | solution.py:78
  105.7 27.9 %reduce-scatter.2.cloned.1.call-done = bf16[1,392,256]{2,1,0:T(8,128)(2,1)} async-done(((bf16[8,392,256]{2,1,0:T(8,128)(2,1)}), bf16[1,392,256]{2,1,0:T(8,128)(2,1)}) %reduce-scatter.2.cloned.1.call-update) | async-done | bytes 200720 | tf_op jit(solution)/shard_map/reduce_scatter | solution.py:431
  133.6 1.4 placed_rows.1
  135.0 21.5 %all_to_all.16.back_ref = bf16[32,16,256]{2,1,0:T(8,128)(2,1)S(1)} all-to-all(bf16[32,16,256]{2,1,0:T(8,128)(2,1)S(1)} %placed_rows.1), channel_id=1, replica_groups=mesh['z'=8,'x'=4,'y'=8,'c'=2] {'z','x'}, dimensions={0} | all-to-all | bytes 524288 | tf_op jit(solution)/shard_map/all_to_all | solution.py:435
  156.5 0.0 copy-done.1
  156.5 0.0 copy-done.2
  156.5 1.0 combine.1
Async XLA Ops:
  7.2 29.8 %copy-start = (bf16[128,1024]{1,0:T(8,128)(2,1)S(1)}, bf16[128,1024]{1,0:T(8,128)(2,1)}, u32[]{:S(2)}) copy-start(bf16[128,1024]{1,0:T(8,128)(2,1)} %param.15) | copy-start | bytes 786436
  7.2 72.5 %all-gather.2.cloned.1.call-start = ((), (), s32[]{:S(2)}) async-start(), calls=%async_computation.4 | async-start | bytes 3538944 | tf_op jit(solution)/shard_map/all_gather | solution.py:417
  39.1 21.4 %all-to-all-start.1 = ((bf16[32,32,256]{2,1,0:T(8,128)(2,1)}), bf16[32,32,256]{2,1,0:T(8,128)(2,1)S(1)}, u32[]{:S(2)}, u32[]{:S(2)}) async-start(bf16[32,32,256]{2,1,0:T(8,128)(2,1)} %bitcast.8), calls=%async_computation.1 | async-start | bytes 1048576 | tf_op jit(solution)/shard_map/all_to_all | solution.py:423
  43.4 90.2 %reduce-scatter.2.cloned.1.call-start = ((), (), s32[]{:S(2)}) async-start(), calls=%async_computation.5 | async-start | bytes 1806336 | tf_op jit(solution)/shard_map/reduce_scatter | solution.py:431
  45.8 15.4 %collective-permute-start = (bf16[3,64,2048]{2,1,0:T(8,128)(2,1)}, bf16[3,64,2048]{2,1,0:T(8,128)(2,1)S(1)}, u32[]{:S(2)}, u32[]{:S(2)}) collective-permute-start(bf16[3,64,2048]{2,1,0:T(8,128)(2,1)} %other_half.1), channel_id=1, source_target_pairs={{0,1},{1,0},{2,3},{3,2},{4,5},{5,4},{6,7},{7,6},{8,9},{9,8},{10,11... | collective-permute-start | bytes 2359304 | tf_op jit(solution)/shard_map/ppermute | solution.py:407
  61.3 18.4 %copy-start.3 = (bf16[3,64,2048]{2,1,0:T(8,128)(2,1)}, bf16[3,64,2048]{2,1,0:T(8,128)(2,1)S(1)}, u32[]{:S(2)}) copy-start(bf16[3,64,2048]{2,1,0:T(8,128)(2,1)S(1)} %collective-permute-done.wr_far) | copy-start | bytes 2359300
  83.9 3.6 %collective-permute-start.1 = (bf16[256,768]{1,0:T(8,128)(2,1)S(1)}, bf16[256,768]{1,0:T(8,128)(2,1)S(1)}, u32[]{:S(2)}, u32[]{:S(2)}) collective-permute-start(bf16[256,768]{1,0:T(8,128)(2,1)S(1)} %forward.1.own_ref), channel_id=1, source_target_pairs={{0,1},{1,0},{2,3},{3,2},{4,5},{5,4},{6,7},{7,6},{8,9},{9,8},{10,11... | collective-permute-start | bytes 1179656 | tf_op jit(solution)/shard_map/ppermute | solution.py:407
  95.6 60.9 %copy-start.1 = (s32[128,2]{0,1:T(2,128)S(1)}, s32[128,2]{0,1:T(2,128)}, u32[]{:S(2)}) copy-start(s32[128,2]{0,1:T(2,128)} %param.10) | copy-start | bytes 3076
  95.6 60.9 %copy-start.2 = (f32[128,2]{0,1:T(2,128)S(1)}, f32[128,2]{0,1:T(2,128)}, u32[]{:S(2)}) copy-start(f32[128,2]{0,1:T(2,128)} %param.11) | copy-start | bytes 3076
  95.6 4.4 %collective-permute-start.2 = (bf16[192,2048]{1,0:T(8,128)(2,1)}, bf16[192,2048]{1,0:T(8,128)(2,1)S(1)}, u32[]{:S(2)}, u32[]{:S(2)}) collective-permute-start(bf16[192,2048]{1,0:T(8,128)(2,1)} %partner_grads.1), channel_id=1, source_target_pairs={{0,1},{1,0},{2,3},{3,2},{4,5},{5,4},{6,7},{7,6},{8,9},{9,8},{10,11... | collective-permute-start | bytes 2359304 | tf_op jit(solution)/shard_map/ppermute | solution.py:407
  100.0 0.9 copy-start.4
Sparse Core Ops, SparseCore 0:
  37.1 42.5 all-gather.1
  91.3 42.2 reduce-scatter.1

commit v6 on v5

--- a/solution.py
+++ b/solution.py
@@ -123,18 +123,17 @@
 
 
 def forward_kernel(
-    c_ref, xg_far, wg_far, wu_far, wd_far, wr_far, out_ref, xg_ref, own_ref, wr_ref, sems
+    c_ref, xg_far, wg_far, wu_far, wd_far, wr_ref, out_ref, xg_ref, own_ref, sems
 ):
     pairs = []
     for y in range(NY):
         pairs.append((xg_far.at[y], xg_ref.at[y]))
-        pairs.append((wr_far.at[:, :, half_lanes(y)], wr_ref.at[:, :, half_lanes(y)]))
         for at, far in enumerate((wg_far, wu_far, wd_far)):
             pairs.append((far.at[:, lanes_of(y, c_ref[0])], own_ref.at[at, :, half_lanes(y)]))
     copies = fetch(pairs, sems)
     total = None
     for y in range(NY):
-        for copy in copies[5 * y : 5 * y + 5]:
+        for copy in copies[4 * y : 4 * y + 4]:
             copy.wait()
         parts = []
         for at in (0, 2, 1):
@@ -161,25 +160,24 @@
         out,
         "forward",
         core=core,
-        far=(xg, wg, wu, wd, wr),
+        far=(xg, wg, wu, wd),
+        near=(wr,),
         scratch=(
             pltpu.VMEM((NY, ROWS, WIDTH), BF16),
             pltpu.VMEM((3, HID, HALF), BF16),
-            pltpu.VMEM((3, HID, HALF), BF16),
-            flags(5 * NY),
+            flags(4 * NY),
         ),
     )[0]
 
 
 def backward_kernel(
-    c_ref, wg_far, wu_far, wr_far, own_ref, got_ref, out_far, left_far,
-    wg_ref, wu_ref, wr_ref, out_ref, left_ref, sems, out_sems,
+    c_ref, wg_far, wu_far, wr_ref, own_ref, got_ref, out_far, left_far,
+    wg_ref, wu_ref, out_ref, left_ref, sems, out_sems,
 ):
     copies = fetch(
         [
             (wg_far, wg_ref),
             (wu_far, wu_ref),
-            (wr_far.at[0:2], wr_ref),
         ],
         sems,
     )
@@ -250,16 +248,15 @@
         out,
         "backward",
         core=core,
-        far=(wg, wu, wr),
-        near=(own, got),
+        far=(wg, wu),
+        near=(wr, own, got),
         far_out=2,
         scratch=(
             pltpu.VMEM((HID, 2 * HALF), BF16),
             pltpu.VMEM((HID, 2 * HALF), BF16),
-            pltpu.VMEM((2, HID, HALF), BF16),
             pltpu.VMEM((NY, BACK, WIDTH), BF16),
             pltpu.VMEM((2, 3 * HID, ROWS), BF16),
-            flags(3),
+            flags(2),
             flags(NY + 1),
         ),
     )

time: 165 us -> 164 us (level)
  no operation moved by 1% of the time
where the time goes in v6:
time: 164 us
  waiting for transfers between devices  63.1 us (38%)
  blocking collectives  50 us (30%)
  Pallas kernels  22.6 us (14%)
  between operations  14.2 us (9%)
  starting transfers between devices  10.2 us (6%)
  local copies, waits for them, and re-layouts  1.92 us (1%)
    all_to_all x1, blocking collectives, shards(): rows = lax.all_to_all(sent, EP, split_axis=0, concat_axis=0, tiled=True)  28.4 us
    reduce_scatter x1, waiting for transfers between devices, shards(): got = lax.psum_scatter(parts, 'y', scatter_dimension=0, tiled=False)  27.8 us
    pallas_call x8, Pallas kernels, kernel_call(): pl.pallas_call(body, in_specs=specs, out_specs=results, out_shape=list(ou...  22.6 us
    all_to_all x1, blocking collectives, shards(): lax.all_to_all(placed_rows(got), EP, split_axis=0, concat_axis=0, tiled=T...  21.6 us
    all_gather x1, waiting for transfers between devices, shards(): xg = lax.all_gather(rows.reshape(ROWS, WIDTH), 'y', axis=0, tiled=False)  18.4 us
    all_to_all x1, waiting for transfers between devices, shards(): lax.all_to_all(shared.reshape(EXPERTS, -1, WIDTH), EP, split_axis=0, conc...  12.8 us
    ppermute x3, starting transfers between devices, core_swap(): return lax.ppermute(value, 'c', [(0, 1), (1, 0)])  5.87 us
    all_to_all x1, starting transfers between devices, shards(): lax.all_to_all(shared.reshape(EXPERTS, -1, WIDTH), EP, split_axis=0, conc...  4.3 us
  transfers between devices with their start and end apart: 6, of which 5 were waited for; matrix products, arithmetic and copies ran while one was open for 2% of the time, Pallas kernels for 7%

profile of v6, /device:TPU:24, one launch (start us, length us, event | category | flops | bytes accessed | tf_op | source)
XLA Modules:
  0.0 163.9 jit_solution(15596054216118972509)
XLA Ops:
  7.2 0.0 copy-start
  7.2 0.0 all-gather.2.cloned.1.call-start
  7.2 1.3 dispatch.1
  8.6 28.4 %all_to_all.15 = bf16[32,24,256]{2,1,0:T(8,128)(2,1)} all-to-all(bf16[32,24,256]{2,1,0:T(8,128)(2,1)S(1)} %dispatch.1), channel_id=1, replica_groups=mesh['z'=8,'x'=4,'y'=8,'c'=2] {'z','x'}, dimensions={0} | all-to-all | bytes 786432 | tf_op jit(solution)/shard_map/all_to_all | solution.py:412
  36.9 0.0 all-gather.2.cloned.1.call-update
  37.0 0.0 copy-done
  37.0 1.2 fusion
  38.1 1.0 copy.15
  39.1 4.3 %all-to-all-start.1 = ((bf16[32,32,256]{2,1,0:T(8,128)(2,1)}), bf16[32,32,256]{2,1,0:T(8,128)(2,1)S(1)}, u32[]{:S(2)}, u32[]{:S(2)}) async-start(bf16[32,32,256]{2,1,0:T(8,128)(2,1)} %bitcast.8), calls=%async_computation.1 | async-start | bytes 1048576 | tf_op jit(solution)/shard_map/all_to_all | solution.py:420
  43.4 0.0 reduce-scatter.2.cloned.1.call-start
  43.5 2.3 %other_half.1 = bf16[3,64,2048]{2,1,0:T(8,128)(2,1)} custom-call(s32[1]{0:T(128)} %bitcast.c_ref, bf16[64,4096]{1,0:T(8,128)(2,1)} %bitcast.21, bf16[64,4096]{1,0:T(8,128)(2,1)} %bitcast.24, bf16[64,4096]{1,0:T(8,128)(2,1)} %bitcast.27), custom_call_target="tpu_custom_call" | custom-call | tf_op jit(solution)/shard_map/other_half/pallas_call | solution.py:78
  45.8 1.9 %collective-permute-start = (bf16[3,64,2048]{2,1,0:T(8,128)(2,1)}, bf16[3,64,2048]{2,1,0:T(8,128)(2,1)S(1)}, u32[]{:S(2)}, u32[]{:S(2)}) collective-permute-start(bf16[3,64,2048]{2,1,0:T(8,128)(2,1)} %other_half.1), channel_id=1, source_target_pairs={{0,1},{1,0},{2,3},{3,2},{4,5},{5,4},{6,7},{7,6},{8,9},{9,8},{10,11... | collective-permute-start | bytes 2359304 | tf_op jit(solution)/shard_map/ppermute | solution.py:404
  47.7 12.8 %all-to-all-done.1 = bf16[32,32,256]{2,1,0:T(8,128)(2,1)S(1)} async-done(((bf16[32,32,256]{2,1,0:T(8,128)(2,1)}), bf16[32,32,256]{2,1,0:T(8,128)(2,1)S(1)}, u32[]{:S(2)}, u32[]{:S(2)}) %all-to-all-start.1) | async-done | bytes 524320 | tf_op jit(solution)/shard_map/all_to_all | solution.py:420
  60.6 0.7 convert_reduce_fusion
  61.3 0.0 collective-permute-done.wr_ref
  61.3 18.4 %all-gather.2.cloned.1.call-done.xg_far = bf16[8,768,256]{2,1,0:T(8,128)(2,1)} async-done(((bf16[1,768,256]{2,1,0:T(8,128)(2,1)}), bf16[8,768,256]{2,1,0:T(8,128)(2,1)}) %all-gather.2.cloned.1.call-update) | async-done | bytes 3145744 | tf_op jit(solution)/shard_map/all_gather | solution.py:414
  79.7 4.1 %forward.1.own_ref = bf16[256,768]{1,0:T(8,128)(2,1)S(1)} custom-call(s32[1]{0:T(128)} %bitcast.c_ref, bf16[8,768,256]{2,1,0:T(8,128)(2,1)} %all-gather.2.cloned.1.call-done.xg_far, bf16[64,4096]{1,0:T(8,128)(2,1)} %bitcast.22, bf16[64,4096]{1,0:T(8,128)(2,1)} %bitcast.25, bf16[64,4096]{1,0:T(8,128)(2,1)} %bitcast.28, ...), custom_call_target="tpu_custom_call" | custom-call | tf_op jit(solution)/shard_map/forward/pallas_call | solution.py:78
  83.8 1.9 %collective-permute-start.1 = (bf16[256,768]{1,0:T(8,128)(2,1)S(1)}, bf16[256,768]{1,0:T(8,128)(2,1)S(1)}, u32[]{:S(2)}, u32[]{:S(2)}) collective-permute-start(bf16[256,768]{1,0:T(8,128)(2,1)S(1)} %forward.1.own_ref), channel_id=1, source_target_pairs={{0,1},{1,0},{2,3},{3,2},{4,5},{5,4},{6,7},{7,6},{8,9},{9,8},{10,11... | collective-permute-start | bytes 1179656 | tf_op jit(solution)/shard_map/ppermute | solution.py:404
  85.7 1.7 %collective-permute-done.1.got_ref = bf16[256,768]{1,0:T(8,128)(2,1)S(1)} collective-permute-done((bf16[256,768]{1,0:T(8,128)(2,1)S(1)}, bf16[256,768]{1,0:T(8,128)(2,1)S(1)}, u32[]{:S(2)}, u32[]{:S(2)}) %collective-permute-start.1) | collective-permute-done | bytes 393248 | tf_op jit(solution)/shard_map/ppermute | solution.py:404
  87.4 3.2 %backward.1 = (bf16[8,392,256]{2,1,0:T(8,128)(2,1)}, bf16[2,192,768]{2,1,0:T(8,128)(2,1)}) custom-call(s32[1]{0:T(128)} %bitcast.c_ref, bf16[64,4096]{1,0:T(8,128)(2,1)} %bitcast.23, bf16[64,4096]{1,0:T(8,128)(2,1)} %bitcast.26, bf16[3,64,2048]{2,1,0:T(8,128)(2,1)S(1)} %collective-permute-done.wr_ref, bf16[256,768]{1,0:T(8,128)(2,1)S(1)} %forward.1.own_ref, ...), custom_call_target="tpu_custom_call" | custom-call | tf_op jit(solution)/shard_map/backward/pallas_call | solution.py:78
  90.6 0.0 reduce-scatter.2.cloned.1.call-update
  90.6 4.5 %partner_grads.1 = bf16[192,2048]{1,0:T(8,128)(2,1)} custom-call(bf16[2,192,768]{2,1,0:T(8,128)(2,1)} %get-tuple-element.33.left_far, bf16[8,768,256]{2,1,0:T(8,128)(2,1)} %all-gather.2.cloned.1.call-done.xg_far), custom_call_target="tpu_custom_call" | custom-call | tf_op jit(solution)/shard_map/partner_grads/pallas_call | solution.py:78
  95.1 0.0 copy-start.1
  95.1 0.0 copy-start.2
  95.1 2.0 %collective-permute-start.2 = (bf16[192,2048]{1,0:T(8,128)(2,1)}, bf16[192,2048]{1,0:T(8,128)(2,1)S(1)}, u32[]{:S(2)}, u32[]{:S(2)}) collective-permute-start(bf16[192,2048]{1,0:T(8,128)(2,1)} %partner_grads.1), channel_id=1, source_target_pairs={{0,1},{1,0},{2,3},{3,2},{4,5},{5,4},{6,7},{7,6},{8,9},{9,8},{10,11... | collective-permute-start | bytes 2359304 | tf_op jit(solution)/shard_map/ppermute | solution.py:404
  97.2 2.3 %collective-permute-done.2.got_far = bf16[192,2048]{1,0:T(8,128)(2,1)S(1)} collective-permute-done((bf16[192,2048]{1,0:T(8,128)(2,1)}, bf16[192,2048]{1,0:T(8,128)(2,1)S(1)}, u32[]{:S(2)}, u32[]{:S(2)}) %collective-permute-start.2) | collective-permute-done | bytes 786464 | tf_op jit(solution)/shard_map/ppermute | solution.py:404
  99.5 0.0 copy-start.3
  99.5 0.9 copy-done.3
  100.4 4.8 %merged_grads.1 = (f32[64,4096]{1,0:T(8,128)}, f32[64,4096]{1,0:T(8,128)}, f32[64,4096]{1,0:T(8,128)}) custom-call(s32[1]{0:T(128)} %bitcast.c_ref, bf16[2,192,768]{2,1,0:T(8,128)(2,1)} %get-tuple-element.33.left_far, bf16[8,768,256]{2,1,0:T(8,128)(2,1)} %all-gather.2.cloned.1.call-done.xg_far, bf16[192,2048]{1,0:T(8,128)(2,1)} %copy-done.3), custom_call_target="tpu_custom_call" | custom-call | tf_op jit(solution)/shard_map/merged_grads/pallas_call | solution.py:78
  105.2 27.8 %reduce-scatter.2.cloned.1.call-done = bf16[1,392,256]{2,1,0:T(8,128)(2,1)} async-done(((bf16[8,392,256]{2,1,0:T(8,128)(2,1)}), bf16[1,392,256]{2,1,0:T(8,128)(2,1)}) %reduce-scatter.2.cloned.1.call-update) | async-done | bytes 200720 | tf_op jit(solution)/shard_map/reduce_scatter | solution.py:428
  133.0 1.4 placed_rows.1
  134.4 21.6 %all_to_all.16.back_ref = bf16[32,16,256]{2,1,0:T(8,128)(2,1)S(1)} all-to-all(bf16[32,16,256]{2,1,0:T(8,128)(2,1)S(1)} %placed_rows.1), channel_id=1, replica_groups=mesh['z'=8,'x'=4,'y'=8,'c'=2] {'z','x'}, dimensions={0} | all-to-all | bytes 524288 | tf_op jit(solution)/shard_map/all_to_all | solution.py:432
  156.0 0.0 copy-done.1
  156.0 0.0 copy-done.2
  156.0 1.0 combine.1
Async XLA Ops:
  7.2 29.8 %copy-start = (bf16[128,1024]{1,0:T(8,128)(2,1)S(1)}, bf16[128,1024]{1,0:T(8,128)(2,1)}, u32[]{:S(2)}) copy-start(bf16[128,1024]{1,0:T(8,128)(2,1)} %param.15) | copy-start | bytes 786436
  7.2 72.5 %all-gather.2.cloned.1.call-start = ((), (), s32[]{:S(2)}) async-start(), calls=%async_computation.4 | async-start | bytes 3538944 | tf_op jit(solution)/shard_map/all_gather | solution.py:414
  39.1 21.4 %all-to-all-start.1 = ((bf16[32,32,256]{2,1,0:T(8,128)(2,1)}), bf16[32,32,256]{2,1,0:T(8,128)(2,1)S(1)}, u32[]{:S(2)}, u32[]{:S(2)}) async-start(bf16[32,32,256]{2,1,0:T(8,128)(2,1)} %bitcast.8), calls=%async_computation.1 | async-start | bytes 1048576 | tf_op jit(solution)/shard_map/all_to_all | solution.py:420
  43.4 89.6 %reduce-scatter.2.cloned.1.call-start = ((), (), s32[]{:S(2)}) async-start(), calls=%async_computation.5 | async-start | bytes 1806336 | tf_op jit(solution)/shard_map/reduce_scatter | solution.py:428
  45.8 15.4 %collective-permute-start = (bf16[3,64,2048]{2,1,0:T(8,128)(2,1)}, bf16[3,64,2048]{2,1,0:T(8,128)(2,1)S(1)}, u32[]{:S(2)}, u32[]{:S(2)}) collective-permute-start(bf16[3,64,2048]{2,1,0:T(8,128)(2,1)} %other_half.1), channel_id=1, source_target_pairs={{0,1},{1,0},{2,3},{3,2},{4,5},{5,4},{6,7},{7,6},{8,9},{9,8},{10,11... | collective-permute-start | bytes 2359304 | tf_op jit(solution)/shard_map/ppermute | solution.py:404
  83.8 3.6 %collective-permute-start.1 = (bf16[256,768]{1,0:T(8,128)(2,1)S(1)}, bf16[256,768]{1,0:T(8,128)(2,1)S(1)}, u32[]{:S(2)}, u32[]{:S(2)}) collective-permute-start(bf16[256,768]{1,0:T(8,128)(2,1)S(1)} %forward.1.own_ref), channel_id=1, source_target_pairs={{0,1},{1,0},{2,3},{3,2},{4,5},{5,4},{6,7},{7,6},{8,9},{9,8},{10,11... | collective-permute-start | bytes 1179656 | tf_op jit(solution)/shard_map/ppermute | solution.py:404
  95.1 60.9 %copy-start.1 = (s32[128,2]{0,1:T(2,128)S(1)}, s32[128,2]{0,1:T(2,128)}, u32[]{:S(2)}) copy-start(s32[128,2]{0,1:T(2,128)} %param.10) | copy-start | bytes 3076
  95.1 60.9 %copy-start.2 = (f32[128,2]{0,1:T(2,128)S(1)}, f32[128,2]{0,1:T(2,128)}, u32[]{:S(2)}) copy-start(f32[128,2]{0,1:T(2,128)} %param.11) | copy-start | bytes 3076
  95.1 4.4 %collective-permute-start.2 = (bf16[192,2048]{1,0:T(8,128)(2,1)}, bf16[192,2048]{1,0:T(8,128)(2,1)S(1)}, u32[]{:S(2)}, u32[]{:S(2)}) collective-permute-start(bf16[192,2048]{1,0:T(8,128)(2,1)} %partner_grads.1), channel_id=1, source_target_pairs={{0,1},{1,0},{2,3},{3,2},{4,5},{5,4},{6,7},{7,6},{8,9},{9,8},{10,11... | collective-permute-start | bytes 2359304 | tf_op jit(solution)/shard_map/ppermute | solution.py:404
  99.5 0.9 copy-start.3
Sparse Core Ops, SparseCore 0:
  37.1 42.5 all-gather.1
  90.7 42.2 reduce-scatter.1
